TPU v7x, 32 devices: a whole 2x2x4 slice. The times are simulated.
32 devices in a mesh: sp: 8 (over z, y), tp: 4 (over x, core).
Axes of the slice: x: 2, y: 2, z: 4, core: 2. Of those that a mesh axis runs over, the one named last changes fastest.
Arguments:
- queries: bfloat16 [1536, 1024], P('sp', 'tp'), may hold values from -0.75 to 0.75
- key_vectors: bfloat16 [1536, 1024], P('sp', 'tp'), may hold values from -0.75 to 0.75
- values_in: bfloat16 [1536, 2048], P('sp', 'tp'), may hold values from -0.75 to 0.75
- log_decay: float32 [1536, 1024], P('sp', 'tp'), may hold values from -1 to 0
- mixed_heads: bfloat16 [1536, 2048], P('sp', 'tp'), may hold values from -6 to 6
- out_proj: bfloat16 [2048, 2048], P('tp'), may hold values from -0.125 to 0.125
- layer_input: bfloat16 [1536, 2048], P('sp'), may hold values from -6 to 6
- cotangent: bfloat16 [1536, 2048], P('sp'), may hold values from -6 to 6
- routes: int32 [1536, 2], P('sp'), may hold values from 0 to 15, all different within a row; in each aligned block of 192 rows (0 to 191, 192 to 383, ...) at most 48 rows name the same one
- route_weight: float32 [1536, 2], P('sp'), may hold values from 0.25 to 2
- gate_weight: bfloat16 [16, 2048, 1024], P('sp', None, 'tp'), may hold values from -0.125 to 0.125
- up_weight: bfloat16 [16, 2048, 1024], P('sp', None, 'tp'), may hold values from -0.125 to 0.125
- down_weight: bfloat16 [16, 1024, 2048], P('sp', 'tp'), may hold values from -0.1875 to 0.1875
Outputs:
- grad_gate: float32 [16, 2048, 1024], P('sp', None, 'tp')
- grad_up: float32 [16, 2048, 1024], P('sp', None, 'tp')
- grad_down: float32 [16, 1024, 2048], P('sp', 'tp')
- grad_proj: float32 [2048, 2048], P('sp', 'tp')
- grad_query: float32 [1536, 1024], P('sp', 'tp')
- grad_key: float32 [1536, 1024], P('sp', 'tp')
- grad_value: float32 [1536, 2048], P('sp', 'tp')
- grad_decay: float32 [1536, 1024], P('sp', 'tp')
Inputs may be any that keep to these rules, and one draw needn't show every extreme that they name: `routes`: in each aligned block of 192 tokens no expert is named by more than 48 pairs, and in some block one expert is named by exactly 48 pairs; the 2 experts of a token differ.
All inputs are finite; a program needn't handle non-finite values.
Results may differ from a plain program's by a relative error of at most 0.015.
Values may be sent and summed in bfloat16 or wider, within the bound.
A program may use at most 192 MiB of HBM per device.

v0:
```python
import jax
import jax.numpy as jnp
from jax import lax
from jax.sharding import PartitionSpec as P

DK = 128
DV = 256


def carried_in(value, axis, join, neutral, backward):
    count, mine = (lax.axis_size(axis), lax.axis_index(axis))
    pieces = jax.tree.map(lambda part: lax.all_gather(part, axis), value)
    if backward:
        pieces = jax.tree.map(lambda part: part[::-1], pieces)
        mine = count - 1 - mine
    so_far = jax.tree.map(
        lambda part, zero: jnp.full_like(part, 0) + jnp.asarray(zero, part.dtype), value, neutral
    )

    def step(position, so_far):
        longer = join(so_far, jax.tree.map(lambda part: part[position], pieces))
        return jax.tree.map(lambda new, old: jnp.where(position < mine, new, old), longer, so_far)

    return lax.fori_loop(0, count - 1, step, so_far)


def local_parts(query_f, key_f, grad_f, pair, decays):
    highest = lax.Precision.HIGHEST
    sigma = query_f.shape[2] ** (-0.5)
    length = query_f.shape[0]
    cum = jnp.cumsum(decays, axis=0)
    total = cum[-1]
    middle = 0.5 * total
    rise = jnp.exp(cum - middle)
    fall = jnp.exp(middle - cum)
    position = jnp.arange(length, dtype=jnp.int32)
    lower = (position[:, None] >= position[None, :])[None]
    score_fwd = (
        jnp.where(
            lower, jnp.einsum("thc,shc->hts", query_f * rise, key_f * fall, precision=highest), 0.0
        )
        * sigma
    )
    score_bwd = (
        jnp.where(
            lower, 0.0, jnp.einsum("thc,shc->hts", query_f * fall, key_f * rise, precision=highest)
        )
        * sigma
    )
    pair_fwd = jnp.where(lower, pair, 0.0)
    pair_bwd = jnp.where(lower, 0.0, pair)
    query_fwd = sigma * rise * jnp.einsum("hts,shc->thc", pair_fwd, key_f * fall, precision=highest)
    query_bwd = sigma * fall * jnp.einsum("hts,shc->thc", pair_bwd, key_f * rise, precision=highest)
    key_fwd = sigma * fall * jnp.einsum("hts,thc->shc", pair_fwd, query_f * rise, precision=highest)
    key_bwd = sigma * rise * jnp.einsum("hts,thc->shc", pair_bwd, query_f * fall, precision=highest)
    value_grad = jnp.einsum("hts,thv->shv", score_fwd + score_bwd, grad_f, precision=highest)
    return (query_fwd, query_bwd, key_fwd, key_bwd, value_grad, cum, total)


def state_terms(query_f, key_f, value_f, grad_f, cum, total):
    highest = lax.Precision.HIGHEST
    head_part = jnp.exp(cum)
    tail = jnp.exp(total - cum)
    kv_fwd = jnp.einsum("shc,shv->hcv", key_f * tail, value_f, precision=highest)
    qo_bwd = jnp.einsum("thc,thv->hcv", query_f * tail, grad_f, precision=highest)
    qo_fwd = jnp.einsum("thc,thv->hcv", query_f * head_part, grad_f, precision=highest)
    kv_bwd = jnp.einsum("shc,shv->hcv", key_f * head_part, value_f, precision=highest)
    return (jnp.exp(total), kv_fwd, qo_bwd, qo_fwd, kv_bwd)


def carried(parts, states, query_f, key_f, value_f, grad_f):
    highest = lax.Precision.HIGHEST
    sigma = query_f.shape[2] ** (-0.5)
    query_fwd, query_bwd, key_fwd, key_bwd, value_grad, cum, total = parts
    kv_low, qo_low, qo_high, kv_high = states
    head_part = jnp.exp(cum)
    tail = jnp.exp(total - cum)
    query_fwd = query_fwd + sigma * head_part * jnp.einsum(
        "thv,hcv->thc", grad_f, kv_low, precision=highest
    )
    query_bwd = query_bwd + sigma * tail * jnp.einsum(
        "thv,hcv->thc", grad_f, kv_high, precision=highest
    )
    key_fwd = key_fwd + sigma * tail * jnp.einsum(
        "shv,hcv->shc", value_f, qo_high, precision=highest
    )
    key_bwd = key_bwd + sigma * head_part * jnp.einsum(
        "shv,hcv->shc", value_f, qo_low, precision=highest
    )
    value_grad = value_grad + sigma * (
        jnp.einsum("shc,hcv->shv", key_f * tail, qo_high, precision=highest)
        + jnp.einsum("shc,hcv->shv", key_f * head_part, qo_low, precision=highest)
    )
    grad_cum = query_f * (query_fwd - query_bwd) - key_f * (key_fwd - key_bwd)
    return (query_fwd + query_bwd, key_fwd + key_bwd, value_grad, grad_cum)


def carry_states(earlier, later):
    return (
        earlier[0] * later[0],
        later[0][..., None] * earlier[1] + later[1],
        later[0][..., None] * earlier[2] + later[2],
    )


def add_terms(earlier, later):
    return earlier + later


def send_back(partial_value):
    row_grad = lax.psum_scatter(
        partial_value.astype(jnp.bfloat16), "tp", scatter_dimension=2, tiled=True
    )
    return lax.all_to_all(row_grad, "sp", split_axis=1, concat_axis=0, tiled=True)


def body(
    queries,
    key_vectors,
    values_in,
    log_decay,
    mixed_heads,
    out_proj,
    layer_input,
    cotangent,
    routes,
    route_weight,
    gate_weight,
    up_weight,
    down_weight,
):
    tok_rows = routes.shape[0]
    top_count = routes.shape[1]
    seq_devices = lax.axis_size("sp")
    tensor_devices = lax.axis_size("tp")
    local_experts = gate_weight.shape[0]
    all_experts = local_experts * seq_devices
    capacity = 2 * tok_rows * top_count // all_experts
    model_width = cotangent.shape[1]
    part_width = model_width // tensor_devices
    column = lax.axis_index("tp") * part_width
    flat_route = routes.reshape(-1)
    onehot = (flat_route[:, None] == jnp.arange(all_experts, dtype=jnp.int32)[None, :]).astype(
        jnp.int32
    )
    rank = jnp.sum((jnp.cumsum(onehot, axis=0) - onehot) * onehot, axis=1)
    place = flat_route * capacity + rank
    token_id = jnp.arange(tok_rows * top_count, dtype=jnp.int32) // top_count
    slot_token = jnp.zeros((all_experts * capacity,), jnp.int32).at[place].set(token_id)
    slot_weight = (
        jnp.zeros((all_experts * capacity,), jnp.float32)
        .at[place]
        .set(route_weight.reshape(-1))
        .reshape(all_experts, capacity)
    )
    input_part = lax.dynamic_slice_in_dim(layer_input, column, part_width, 1)[slot_token]
    cot_part = lax.dynamic_slice_in_dim(cotangent, column, part_width, 1)[slot_token]
    rows_part, cot_arrived, expert_weight = (
        lax.all_to_all(
            input_part.reshape(all_experts, capacity, part_width),
            "sp",
            split_axis=0,
            concat_axis=1,
            tiled=True,
        ),
        lax.all_to_all(
            cot_part.reshape(all_experts, capacity, part_width),
            "sp",
            split_axis=0,
            concat_axis=1,
            tiled=True,
        ),
        lax.all_to_all(
            slot_weight.astype(jnp.bfloat16), "sp", split_axis=0, concat_axis=1, tiled=True
        ).astype(slot_weight.dtype),
    )
    expert_rows, expert_cot = (
        lax.all_gather(rows_part, "tp", axis=2, tiled=True),
        lax.all_gather(cot_arrived, "tp", axis=2, tiled=True),
    )
    pre_gate = jnp.einsum(
        "erd,edf->erf", expert_rows, gate_weight, preferred_element_type=jnp.float32
    )
    pre_up = jnp.einsum("erd,edf->erf", expert_rows, up_weight, preferred_element_type=jnp.float32)
    weighted = (expert_weight[:, :, None] * expert_cot).astype(jnp.bfloat16)
    d_act = jnp.einsum("erd,efd->erf", weighted, down_weight, preferred_element_type=jnp.float32)
    sigmoid_gate = jax.nn.sigmoid(pre_gate)
    silu_gate = pre_gate * sigmoid_gate
    act = (silu_gate * pre_up).astype(jnp.bfloat16)
    d_gate = (d_act * pre_up * sigmoid_gate * (1.0 + pre_gate * (1.0 - sigmoid_gate))).astype(
        jnp.bfloat16
    )
    d_up = (d_act * silu_gate).astype(jnp.bfloat16)
    partial_value = jnp.einsum(
        "erf,edf->erd", d_gate, gate_weight, preferred_element_type=jnp.float32
    ) + jnp.einsum("erf,edf->erd", d_up, up_weight, preferred_element_type=jnp.float32)
    grad_gate, grad_up, grad_down = (
        jnp.einsum("erd,erf->edf", expert_rows, d_gate, preferred_element_type=jnp.float32),
        jnp.einsum("erd,erf->edf", expert_rows, d_up, preferred_element_type=jnp.float32),
        jnp.einsum("erf,erd->efd", act, weighted, preferred_element_type=jnp.float32),
    )
    returned = send_back(partial_value)
    gathered = returned.reshape(all_experts * capacity, part_width)[place].reshape(
        tok_rows, top_count, part_width
    )
    own_cot = lax.dynamic_slice_in_dim(cotangent, column, part_width, 1)
    token_part = (
        own_cot.astype(jnp.float32) + jnp.sum(gathered.astype(jnp.float32), axis=1)
    ).astype(jnp.bfloat16)
    token_grad = lax.all_gather(token_part, "tp", axis=1, tiled=True)
    grad_proj = lax.psum_scatter(
        lax.dot_general(
            token_grad, mixed_heads, (((0,), (0,)), ((), ())), preferred_element_type=jnp.float32
        ),
        "sp",
        scatter_dimension=0,
        tiled=True,
    )
    head_grad = lax.dot_general(
        token_grad, out_proj, (((1,), (1,)), ((), ())), preferred_element_type=jnp.float32
    )
    heads_local = queries.shape[1] // DK
    query_f = queries.reshape(tok_rows, heads_local, DK).astype(jnp.float32)
    key_f = key_vectors.reshape(tok_rows, heads_local, DK).astype(jnp.float32)
    value_f = values_in.reshape(tok_rows, heads_local, DV).astype(jnp.float32)
    grad_f = head_grad.reshape(tok_rows, heads_local, DV)
    decays = log_decay.reshape(tok_rows, heads_local, DK)
    pair = jnp.einsum("thv,shv->hts", grad_f, value_f, precision=lax.Precision.HIGHEST)
    parts = local_parts(query_f, key_f, grad_f, pair, decays)
    decay_all, kv_fwd, qo_bwd, qo_fwd, kv_bwd = state_terms(
        query_f, key_f, value_f, grad_f, parts[5], parts[6]
    )
    identity = (
        jnp.ones((heads_local, DK), jnp.float32),
        jnp.zeros((heads_local, DK, DV), jnp.float32),
        jnp.zeros((heads_local, DK, DV), jnp.float32),
    )
    from_lower = carried_in((decay_all, kv_fwd, qo_bwd), "sp", carry_states, identity, False)
    from_higher = carried_in((decay_all, qo_fwd, kv_bwd), "sp", carry_states, identity, True)
    query_grad, key_grad, value_grad, grad_cum = carried(
        parts,
        (from_lower[1], from_lower[2], from_higher[1], from_higher[2]),
        query_f,
        key_f,
        value_f,
        grad_f,
    )
    grad_cum = grad_cum.reshape(tok_rows, heads_local * DK)
    reverse_sum = jnp.flip(jnp.cumsum(jnp.flip(grad_cum, 0), axis=0), 0)
    beyond = carried_in(reverse_sum[0], "sp", add_terms, jnp.zeros_like(reverse_sum[0]), True)
    grad_decay = reverse_sum + beyond[None, :]
    return (
        grad_gate,
        grad_up,
        grad_down,
        grad_proj,
        query_grad.reshape(tok_rows, heads_local * DK),
        key_grad.reshape(tok_rows, heads_local * DK),
        value_grad.reshape(tok_rows, heads_local * DV),
        grad_decay,
    )


def solution(mesh):
    return jax.shard_map(
        body,
        mesh=mesh,
        in_specs=(
            P("sp", "tp"),
            P("sp", "tp"),
            P("sp", "tp"),
            P("sp", "tp"),
            P("sp", "tp"),
            P("tp", None),
            P("sp", None),
            P("sp", None),
            P("sp", None),
            P("sp", None),
            P("sp", None, "tp"),
            P("sp", None, "tp"),
            P("sp", "tp", None),
        ),
        out_specs=(
            P("sp", None, "tp"),
            P("sp", None, "tp"),
            P("sp", "tp", None),
            P("sp", "tp"),
            P("sp", "tp"),
            P("sp", "tp"),
            P("sp", "tp"),
            P("sp", "tp"),
        ),
        check_vma=False,
    )
```

profile of v0, /device:TPU:0, one launch (start us, length us, event | category | flops | bytes accessed | tf_op | source)
XLA Modules:
  0.0 444.8 jit_solution(18050371921878534155)
XLA Ops:
  11.5 2.9 scatter_custom_fusion
  15.5 2.7 gather_fusion
  18.2 27.3 %all_to_all.61 = bf16[16,48,512]{2,1,0:T(8,128)(2,1)S(1)} all-to-all(bf16[16,48,512]{2,1,0:T(8,128)(2,1)S(1)} %bitcast.215), channel_id=1, replica_groups=mesh['sp'=8,'tp'=4] {'sp'}, dimensions={0} | all-to-all | bytes 1572864 | tf_op jit(solution)/shard_map/all_to_all | solution.py:159
  46.5 2.7 gather_fusion.1
  49.2 23.2 %all_to_all.62 = bf16[16,48,512]{2,1,0:T(8,128)(2,1)S(1)} all-to-all(bf16[16,48,512]{2,1,0:T(8,128)(2,1)S(1)} %bitcast.216), channel_id=1, replica_groups=mesh['sp'=8,'tp'=4] {'sp'}, dimensions={0} | all-to-all | bytes 1572864 | tf_op jit(solution)/shard_map/all_to_all | solution.py:166
  73.7 2.9 scatter_custom_fusion.1
  76.7 9.9 %all_to_all.63 = bf16[8,2,48]{2,1,0:T(2,128)(2,1)S(1)} all-to-all(bf16[8,2,48]{2,1,0:T(2,128)(2,1)S(1)} %convert_element_type.73), channel_id=1, replica_groups=mesh['sp'=8,'tp'=4] {'sp'}, dimensions={0} | all-to-all | bytes 3072 | tf_op jit(solution)/shard_map/all_to_all | solution.py:173
  86.7 3.7 fusion.113
  90.4 1.9 fusion.114
  92.3 12.5 %all-gather.14.cloned.1.call-done = bf16[2,384,2048]{2,1,0:T(8,128)(2,1)} async-done(((bf16[2,384,512]{2,1,0:T(8,128)(2,1)}), bf16[2,384,2048]{2,1,0:T(8,128)(2,1)}) %all-gather.14.cloned.1.call-update) | async-done | bytes 3145744 | tf_op jit(solution)/shard_map/all_gather | solution.py:179
  104.8 3.9 multiply_convert_fusion.4
  110.6 2.7 add_convert_fusion
  115.2 1.3 fusion.103
  117.7 33.5 %reduce-scatter.3.cloned.1.call-done = bf16[2,384,512]{2,1,0:T(8,128)(2,1)} async-done(((bf16[2,384,2048]{2,1,0:T(8,128)(2,1)}), bf16[2,384,512]{2,1,0:T(8,128)(2,1)}) %reduce-scatter.3.cloned.1.call-update) | async-done | bytes 786448 | tf_op jit(solution)/shard_map/reduce_scatter | solution.py:111
  151.2 2.8 copy.193
  154.0 5.5 %all-to-all-start.3 = ((bf16[2,384,512]{2,0,1:T(2,128)(2,1)}), bf16[2,384,512]{2,0,1:T(2,128)(2,1)S(1)}, u32[]{:S(2)}, u32[]{:S(2)}) async-start(bf16[2,384,512]{2,0,1:T(2,128)(2,1)} %copy.193), calls=%async_computation.4 | async-start | bytes 1572864 | tf_op jit(solution)/shard_map/all_to_all | solution.py:114
  159.6 24.0 %all-to-all-done.3 = bf16[2,384,512]{2,0,1:T(2,128)(2,1)S(1)} async-done(((bf16[2,384,512]{2,0,1:T(2,128)(2,1)}), bf16[2,384,512]{2,0,1:T(2,128)(2,1)S(1)}, u32[]{:S(2)}, u32[]{:S(2)}) %all-to-all-start.3) | async-done | bytes 786464 | tf_op jit(solution)/shard_map/all_to_all | solution.py:114
  183.8 2.1 gather_fusion.2
  187.4 8.7 %all_gather.44 = bf16[192,2048]{1,0:T(8,128)(2,1)S(1)} all-gather(bf16[192,512]{1,0:T(8,128)(2,1)S(1)} %add_convert_fusion.1), channel_id=1, replica_groups=mesh['sp'=8,'tp'=4] {'tp'}, dimensions={1}, use_global_device_ids=true | all-gather | bytes 983040 | tf_op jit(solution)/shard_map/all_gather | solution.py:210
  196.1 2.4 fusion.119
  198.5 1.4 fusion.16
  201.2 1.4 fusion.20
  202.8 17.9 %all_gather.45 = f32[8,2,128]{2,1,0:T(2,128)S(1)} all-gather(f32[1,2,128]{2,1,0:T(2,128)S(1)} %get-tuple-element.507), channel_id=1, replica_groups=mesh['sp'=8,'tp'=4] {'sp'}, dimensions={0}, use_global_device_ids=true | all-gather | bytes 9216 | tf_op jit(solution)/shard_map/all_gather | solution.py:12
  221.2 1.3 fusion.7
  222.5 3.1 rev.21
  225.6 5.6 %fusion.116 = f32[2,2048,256]{2,1,0:T(8,128)} fusion(bf16[2,384,2048]{2,1,0:T(8,128)(2,1)} %all-gather.12.cloned.1.call-done, bf16[2,384,256]{2,1,0:T(8,128)(2,1)} %copy-done.24), kind=kOutput, calls=%fused_computation.178 | convolution fusion | flops 805306368 | bytes 7733248 | tf_op jit(solution)/shard_map/erd,erf->edf/dot_general | solution.py:199
  231.2 3.5 fusion.115
  234.7 3.4 fusion.4
  238.5 1.6 fusion.24
  240.1 1.2 fusion.26
  241.2 1.6 fusion.28
  242.9 1.2 fusion.30
  245.0 2.7 fusion.118
  247.8 3.1 rev.20
  250.9 8.4 %while.47 = (s32[]{:T(128)}, f32[2,128,256]{2,1,0:T(8,128)S(1)}, f32[2,128,256]{2,1,0:T(8,128)S(1)}, s32[]{:T(128)}, f32[8,2,128]{2,1,0:T(2,128)S(1)}, /*index=5...) while((s32[]{:T(128)}, f32[2,128,256]{2,1,0:T(8,128)S(1)}, ...), condition=%wide.region_13.14_spmd.clone, body=%wide.region_12.13_spmd.clone.sunk | while | flops 524292 | bytes 1576057 | solution.py:24
  252.1 1.2 fusion.147
  254.5 1.2 fusion.147
  255.8 1.2 fusion.147
  258.2 1.2 fusion.147
  260.4 36.1 %all-gather.16.cloned.1.call-done = f32[16,128,256]{2,1,0:T(8,128)} async-done(((f32[2,128,256]{2,1,0:T(8,128)}), f32[16,128,256]{2,1,0:T(8,128)}) %all-gather.16.cloned.1.call-update) | async-done | bytes 2097168 | tf_op jit(solution)/shard_map/all_gather | solution.py:12
  296.5 49.7 %all-gather.18.cloned.1.call-done = f32[16,128,256]{2,1,0:T(8,128)} async-done(((f32[2,128,256]{2,1,0:T(8,128)}), f32[16,128,256]{2,1,0:T(8,128)}) %all-gather.18.cloned.1.call-update) | async-done | bytes 2097168 | tf_op jit(solution)/shard_map/all_gather | solution.py:12
  346.3 8.5 %while.46 = (s32[]{:T(128)}, f32[2,128,256]{2,1,0:T(8,128)S(1)}, f32[2,128,256]{2,1,0:T(8,128)S(1)}, s32[]{:T(128)}, f32[8,2,128]{2,1,0:T(2,128)S(1)}, /*index=5...) while((s32[]{:T(128)}, f32[2,128,256]{2,1,0:T(8,128)S(1)}, ...), condition=%wide.region_11.12_spmd.clone, body=%wide.region_10.11_spmd.clone.sunk | while | flops 524292 | bytes 1576057 | solution.py:24
  346.3 1.2 fusion.146
  356.2 3.8 multiply_subtract_fusion
  362.2 2.9 rev.23
  365.8 18.9 %all-gather.4 = f32[8,1,256]{2,1,0:T(1,128)S(1)} all-gather(f32[1,1,256]{2,1,0:T(1,128)S(1)} %slice_bitcast_fusion.2), channel_id=1, replica_groups=mesh['sp'=8,'tp'=4] {'sp'}, dimensions={0}, use_global_device_ids=true | all-gather | bytes 9216 | tf_op jit(solution)/shard_map/all_gather | solution.py:12
  388.5 1.6 broadcast_add_fusion.2
  390.1 47.3 %reduce-scatter.5.cloned.1.call-done = f32[256,512]{1,0:T(8,128)} async-done(((f32[2048,512]{1,0:T(8,128)}), f32[256,512]{1,0:T(8,128)}) %reduce-scatter.5.cloned.1.call-update) | async-done | bytes 524304 | tf_op jit(solution)/shard_map/reduce_scatter | solution.py:211
  (214 shorter events, 36.3 us)
Async XLA Ops:
  8.0 82.4 %copy-start = (bf16[2,2048,256]{2,1,0:T(8,128)(2,1)S(1)}, bf16[2,2048,256]{2,1,0:T(8,128)(2,1)}, u32[]{:S(2)}) copy-start(bf16[2,2048,256]{2,1,0:T(8,128)(2,1)} %param.29) | copy-start | bytes 6291460
  8.0 78.7 %all-gather.12.cloned.1.call-start = ((), (), s32[]{:S(2)}) async-start(), calls=%async_computation.6 | async-start | bytes 3932160 | tf_op jit(solution)/shard_map/all_gather | solution.py:178
  46.4 58.3 %all-gather.14.cloned.1.call-start = ((), (), s32[]{:S(2)}) async-start(), calls=%async_computation.7 | async-start | bytes 3932160 | tf_op jit(solution)/shard_map/all_gather | solution.py:179
  49.2 24.2 %copy-start.38 = (f32[192,2]{0,1:T(2,128)S(1)}, f32[192,2]{0,1:T(2,128)}, u32[]{:S(2)}) copy-start(f32[192,2]{0,1:T(2,128)} %param.28) | copy-start | bytes 4612
  73.3 77.9 %reduce-scatter.3.cloned.1.call-start = ((), (), s32[]{:S(2)}) async-start(), calls=%async_computation.8 | async-start | bytes 3932160 | tf_op jit(solution)/shard_map/reduce_scatter | solution.py:111
  86.7 3.7 copy-start.2
  90.4 18.3 %copy-start.7 = (f32[2,384,256]{2,1,0:T(8,128)}, f32[2,384,256]{2,1,0:T(8,128)S(1)}, u32[]{:S(2)}) copy-start(f32[2,384,256]{2,1,0:T(8,128)S(1)} %fusion.113) | copy-start | bytes 2359300
  108.7 1.1 copy-start.22
  108.7 1.1 copy-start.24
  108.8 1.9 copy-start.4
  113.3 0.9 copy-start.35
  113.3 1.6 copy-start.36
  113.3 1.8 copy-start.37
  113.3 3.2 copy-start.5
  113.4 109.2 %all-gather.22.cloned.1.call-start = ((), (), s32[]{:S(2)}) async-start(), calls=%async_computation.13 | async-start | bytes 2359296 | tf_op jit(solution)/shard_map/all_gather | solution.py:12
  114.9 39.1 %copy-start.20 = (f32[128,2,2,128]{0,1,3,2:T(2,128)}, f32[128,2,2,128]{0,1,3,2:T(2,128)S(1)}, u32[]{:S(2)}) copy-start(f32[128,2,2,128]{0,1,3,2:T(2,128)S(1)} %copy.197) | copy-start | bytes 786436
  115.1 39.0 %copy-start.16 = (f32[192,2,128]{2,1,0:T(2,128)}, f32[192,2,128]{2,1,0:T(2,128)S(1)}, u32[]{:S(2)}) copy-start(f32[192,2,128]{2,1,0:T(2,128)S(1)} %reshape.171) | copy-start | bytes 589828
  115.2 68.5 %copy-start.18 = (f32[192,2,128]{2,1,0:T(2,128)}, f32[192,2,128]{2,1,0:T(2,128)S(1)}, u32[]{:S(2)}) copy-start(f32[192,2,128]{2,1,0:T(2,128)S(1)} %reshape.172) | copy-start | bytes 589828
  116.5 83.5 %copy-start.14 = (f32[192,2,128]{2,1,0:T(2,128)}, f32[192,2,128]{2,1,0:T(2,128)S(1)}, u32[]{:S(2)}) copy-start(f32[192,2,128]{2,1,0:T(2,128)S(1)} %get-tuple-element.502) | copy-start | bytes 589828
  116.5 104.2 %copy-start.10 = (f32[192,2,128]{2,1,0:T(2,128)}, f32[192,2,128]{2,1,0:T(2,128)S(1)}, u32[]{:S(2)}) copy-start(f32[192,2,128]{2,1,0:T(2,128)S(1)} %get-tuple-element.504) | copy-start | bytes 589828
  116.5 104.2 %copy-start.12 = (f32[192,2,128]{2,1,0:T(2,128)}, f32[192,2,128]{2,1,0:T(2,128)S(1)}, u32[]{:S(2)}) copy-start(f32[192,2,128]{2,1,0:T(2,128)S(1)} %get-tuple-element.497) | copy-start | bytes 589828
  154.0 29.6 %all-to-all-start.3 = ((bf16[2,384,512]{2,0,1:T(2,128)(2,1)}), bf16[2,384,512]{2,0,1:T(2,128)(2,1)S(1)}, u32[]{:S(2)}, u32[]{:S(2)}) async-start(bf16[2,384,512]{2,0,1:T(2,128)(2,1)} %copy.193), calls=%async_computation.4 | async-start | bytes 1572864 | tf_op jit(solution)/shard_map/all_to_all | solution.py:114
  159.6 88.2 %all-gather.20.cloned.1.call-start = ((), (), s32[]{:S(2)}) async-start(), calls=%async_computation.12 | async-start | bytes 2359296 | tf_op jit(solution)/shard_map/all_gather | solution.py:12
  187.3 11.2 %copy-start.28 = (f32[192,2,128]{2,1,0:T(2,128)S(1)}, f32[192,2,128]{2,1,0:T(2,128)}, u32[]{:S(2)}) copy-start(f32[192,2,128]{2,1,0:T(2,128)} %get-tuple-element.500) | copy-start | bytes 589828
  187.4 13.8 %copy-start.27 = (f32[192,2,128]{2,1,0:T(2,128)S(1)}, f32[192,2,128]{2,1,0:T(2,128)}, u32[]{:S(2)}) copy-start(f32[192,2,128]{2,1,0:T(2,128)} %get-tuple-element.501) | copy-start | bytes 589828
  199.9 96.6 %all-gather.16.cloned.1.call-start = ((), (), s32[]{:S(2)}) async-start(), calls=%async_computation.10 | async-start | bytes 2359296 | tf_op jit(solution)/shard_map/all_gather | solution.py:12
  201.2 145.1 %all-gather.18.cloned.1.call-start = ((), (), s32[]{:S(2)}) async-start(), calls=%async_computation.11 | async-start | bytes 2359296 | tf_op jit(solution)/shard_map/all_gather | solution.py:12
  202.7 234.8 %reduce-scatter.5.cloned.1.call-start = ((), (), s32[]{:S(2)}) async-start(), calls=%async_computation.9 | async-start | bytes 4718592 | tf_op jit(solution)/shard_map/reduce_scatter | solution.py:211
  225.6 5.6 %copy-start.3 = (bf16[2,384,2048]{2,1,0:T(8,128)(2,1)S(1)}, bf16[2,384,2048]{2,1,0:T(8,128)(2,1)}, u32[]{:S(2)}) copy-start(bf16[2,384,2048]{2,1,0:T(8,128)(2,1)} %all-gather.12.cloned.1.call-done) | copy-start | bytes 9437188
  225.6 5.6 %copy-start.23 = (bf16[2,384,256]{2,1,0:T(8,128)(2,1)S(1)}, bf16[2,384,256]{2,1,0:T(8,128)(2,1)}, u32[]{:S(2)}) copy-start(bf16[2,384,256]{2,1,0:T(8,128)(2,1)} %copy-done.22) | copy-start | bytes 1179652
  231.2 3.5 copy-start.6
  231.2 3.5 copy-start.8
  231.2 3.5 copy-start.9
  234.7 3.8 copy-start.13
  234.7 5.4 %copy-start.11 = (f32[192,2,128]{2,1,0:T(2,128)S(1)}, f32[192,2,128]{2,1,0:T(2,128)}, u32[]{:S(2)}) copy-start(f32[192,2,128]{2,1,0:T(2,128)} %copy-done.10) | copy-start | bytes 589828
  238.1 5.9 %copy-start.25 = (f32[2,192,192]{2,1,0:T(8,128)S(1)}, f32[2,192,192]{2,1,0:T(8,128)}, u32[]{:S(2)}) copy-start(f32[2,192,192]{2,1,0:T(8,128)} %fusion.7) | copy-start | bytes 884740
  238.1 6.9 %copy-start.34 = (bf16[192,512]{1,0:T(8,128)(2,1)S(1)}, bf16[192,512]{1,0:T(8,128)(2,1)}, u32[]{:S(2)}) copy-start(bf16[192,512]{1,0:T(8,128)(2,1)} %param.23) | copy-start | bytes 589828
  346.3 9.9 %copy-start.17 = (f32[192,2,128]{2,1,0:T(2,128)S(1)}, f32[192,2,128]{2,1,0:T(2,128)}, u32[]{:S(2)}) copy-start(f32[192,2,128]{2,1,0:T(2,128)} %copy-done.16) | copy-start | bytes 589828
  346.3 9.9 %copy-start.19 = (f32[192,2,128]{2,1,0:T(2,128)S(1)}, f32[192,2,128]{2,1,0:T(2,128)}, u32[]{:S(2)}) copy-start(f32[192,2,128]{2,1,0:T(2,128)} %copy-done.18) | copy-start | bytes 589828
  346.3 9.9 %copy-start.21 = (f32[128,2,2,128]{0,1,3,2:T(2,128)S(1)}, f32[128,2,2,128]{0,1,3,2:T(2,128)}, u32[]{:S(2)}) copy-start(f32[128,2,2,128]{0,1,3,2:T(2,128)} %copy-done.20) | copy-start | bytes 786436
  346.3 9.9 %copy-start.29 = (f32[2,128,192]{1,2,0:T(8,128)S(1)}, f32[2,128,192]{1,2,0:T(8,128)}, u32[]{:S(2)}) copy-start(f32[2,128,192]{1,2,0:T(8,128)} %fusion.24) | copy-start | bytes 589828
  356.2 28.5 %copy-start.15 = (f32[192,2,128]{2,1,0:T(2,128)S(1)}, f32[192,2,128]{2,1,0:T(2,128)}, u32[]{:S(2)}) copy-start(f32[192,2,128]{2,1,0:T(2,128)} %copy-done.14) | copy-start | bytes 589828
  360.8 0.7 copy-start.26
  361.5 75.9 %copy-start.1 = (bf16[2,2048,256]{2,1,0:T(8,128)(2,1)S(1)}, bf16[2,2048,256]{2,1,0:T(8,128)(2,1)}, u32[]{:S(2)}) copy-start(bf16[2,2048,256]{2,1,0:T(8,128)(2,1)} %param.29) | copy-start | bytes 6291460
  384.7 1.9 copy-start.32
  384.7 1.9 copy-start.33
  384.7 2.6 copy-start.30
  384.7 2.6 copy-start.31
Sparse Core Ops, SparseCore 0:
  46.6 27.4 all-gather.11
  76.2 28.4 all-gather.13
  113.5 37.7 reduce-scatter.2
Sparse Core Ops, SparseCore 1:
  117.8 52.3 all-gather.21
  200.0 46.8 all-gather.19
  248.9 47.5 all-gather.15
  298.7 47.5 all-gather.17
  350.5 86.9 reduce-scatter.4
where the time goes:
time: 446 us; the launch traced here: 445 us
  waiting for transfers between devices  203 us (46%)
  blocking collectives  106 us (24%)
  matrix products  47.9 us (11%)
  local copies, waits for them, and re-layouts  38 us (9%)
  other arithmetic  26.8 us (6%)
  between operations  16.2 us (4%)
  starting transfers between devices  6.03 us (1%)
    all_gather x4, waiting for transfers between devices, carried_in(): pieces = jax.tree.map(lambda part: lax.all_gather(part, axis), value)  85.9 us
    reduce_scatter x1, waiting for transfers between devices, body(): lax.psum_scatter(lax.dot_general(token_grad, mixed_heads, (((0,), (0,)),...  47.3 us
    all_gather x2, blocking collectives, carried_in(): pieces = jax.tree.map(lambda part: lax.all_gather(part, axis), value)  36.8 us
    reduce_scatter x1, waiting for transfers between devices, send_back(): lax.psum_scatter(partial_value.astype(jnp.bfloat16), 'tp', scatter_dimens...  33.5 us
    all_to_all x1, blocking collectives, body(): lax.all_to_all(input_part.reshape(all_experts, capacity, part_width), 'sp...  27.3 us
    all_to_all x1, waiting for transfers between devices, send_back(): lax.all_to_all(row_grad, 'sp', split_axis=1, concat_axis=0, tiled=True)  24 us
    all_to_all x1, blocking collectives, body(): lax.all_to_all(cot_part.reshape(all_experts, capacity, part_width), 'sp',...  23.2 us
    select_n x21, other arithmetic, step(): jnp.where(position < mine, new, old)  16.5 us
  transfers between devices with their start and end apart: 9, of which 6 were waited for; matrix products, arithmetic and copies ran while one was open for 21% of the time, Pallas kernels for 0%

commit v1 on v0

v1 whole, which is shorter than its diff:
```python
import functools

import jax
import jax.numpy as jnp
from jax import lax
from jax.experimental import pallas as pl
from jax.experimental.pallas import tpu as pltpu
from jax.sharding import PartitionSpec as P

DK = 128
DV = 256
VMEM = pltpu.VMEM
ANY = pl.ANY


def remote(source, target, send_sem, recv_sem, device):
    return pltpu.make_async_remote_copy(
        src_ref=source,
        dst_ref=target,
        send_sem=send_sem,
        recv_sem=recv_sem,
        device_id=device,
        device_id_type=pl.DeviceIdType.MESH,
    )


def greet(seq, tensor, s, tp_peers):
    barrier = pltpu.get_barrier_semaphore()
    for d in range(1, seq):
        pl.semaphore_signal(
            barrier,
            inc=1,
            device_id={"sp": lax.rem(s + d, seq)},
            device_id_type=pl.DeviceIdType.MESH,
        )
    for peer in tp_peers:
        pl.semaphore_signal(
            barrier, inc=1, device_id={"tp": peer}, device_id_type=pl.DeviceIdType.MESH
        )
    pl.semaphore_wait(barrier, seq - 1 + len(tp_peers))


def neighbours(tensor):
    t = lax.axis_index("tp")
    beside = t + 1 - 2 * lax.rem(t, 2)
    across = lax.rem(t + tensor // 2, tensor)
    return t, beside, across


def dispatch_kernel(
    seq,
    tensor,
    width,
    rows_ref,
    cot_ref,
    total_ref,
    state_ref,
    rows_out,
    cot_out,
    total_out,
    state_out,
    sp_send,
    sp_recv,
    tp_send,
    tp_recv,
    small_send,
    small_recv,
    own_sem,
):
    s = lax.axis_index("sp")
    t, beside, across = neighbours(tensor)
    ins, outs = (rows_ref, cot_ref), (rows_out, cot_out)
    greet(seq, tensor, s, (beside, across))

    def place(a, block, part):
        return outs[a].at[:, block, :, pl.ds(pl.multiple_of(part * width, width), width)]

    def spread(a, d):
        to = lax.rem(s + d, seq)
        return remote(
            ins[a].at[to], place(a, s, t), sp_send.at[a, d], sp_recv.at[a, d], {"sp": to}
        )

    def origin(d):
        return lax.rem(s - d + seq, seq)

    def forward(a, d, way):
        block = origin(d)
        part = across if way == 2 else t
        source = ins[a].at[s] if d == 0 and way != 2 else place(a, block, part)
        return remote(
            source,
            place(a, block, part),
            tp_send.at[way, a, d],
            tp_recv.at[way, a, d],
            {"tp": across if way == 1 else beside},
        )

    def small(d, which):
        to = lax.rem(s + d, seq)
        if which == 0:
            source, target = total_ref, total_out.at[s]
        else:
            source, target = state_ref.at[jnp.where(to > s, 0, 1)], state_out.at[s]
        return remote(
            source, target, small_send.at[which, d], small_recv.at[which, d], {"sp": to}
        )

    for d in range(1, seq):
        for a in range(2):
            spread(a, d).start()
    own = [
        pltpu.make_async_copy(ins[a].at[s], place(a, s, t), own_sem.at[a]) for a in range(2)
    ] + [
        pltpu.make_async_copy(total_ref, total_out.at[s], own_sem.at[2]),
        pltpu.make_async_copy(state_ref.at[0], state_out.at[s], own_sem.at[3]),
    ]
    for copy in own:
        copy.start()
    for a in range(2):
        forward(a, 0, 1).start()
        forward(a, 0, 0).start()
    for d in range(1, seq):
        small(d, 0).start()
        small(d, 1).start()
    lag = 2
    for d in range(1, seq + lag):
        if d < seq:
            for a in range(2):
                spread(a, d).wait_recv()
                forward(a, d, 1).start()
                forward(a, d, 0).start()
        if d >= lag:
            for a in range(2):
                forward(a, d - lag, 1).wait_recv()
                forward(a, d - lag, 2).start()
    for d in range(seq):
        for a in range(2):
            if d:
                spread(a, d).wait_send()
            forward(a, d, 0).wait()
            forward(a, d, 1).wait_send()
            forward(a, d, 2).wait()
        if d:
            small(d, 0).wait()
            small(d, 1).wait()
    for copy in own:
        copy.wait()


def return_kernel(
    seq,
    tensor,
    width,
    part_ref,
    cot_ref,
    pick_ref,
    mixed_ref,
    token_out,
    mixed_out,
    arrived,
    summed,
    back,
    total,
    red_send,
    red_recv,
    sp_send,
    sp_recv,
    mix_send,
    mix_recv,
    tok_send,
    tok_recv,
    own_sem,
):
    s = lax.axis_index("sp")
    t, beside, across = neighbours(tensor)
    experts = part_ref.shape[0]
    greet(seq, tensor, s, tuple(lax.rem(t + u, tensor) for u in range(1, tensor)))

    def columns(part):
        return pl.ds(pl.multiple_of(part * width, width), width)

    def reduce(d, u):
        block = lax.rem(s + d, seq)
        to = lax.rem(t + u, tensor)
        return remote(
            part_ref.at[:, block, :, columns(to)],
            arrived.at[u - 1, d],
            red_send.at[u - 1, d],
            red_recv.at[u - 1, d],
            {"tp": to},
        )

    def give(d):
        to = lax.rem(s + d, seq)
        return remote(summed.at[d], back.at[d], sp_send.at[d], sp_recv.at[d], {"sp": to})

    def mix(d):
        to = lax.rem(s + d, seq)
        return remote(
            mixed_ref, mixed_out.at[s], mix_send.at[d], mix_recv.at[d], {"sp": to}
        )

    def token(way):
        part = across if way == 2 else t
        return remote(
            token_out.at[part],
            token_out.at[part],
            tok_send.at[way],
            tok_recv.at[way],
            {"tp": across if way == 1 else beside},
        )

    order = list(range(1, seq)) + [0]
    for d in order:
        for u in range(1, tensor):
            reduce(d, u).start()
    own = pltpu.make_async_copy(mixed_ref, mixed_out.at[s], own_sem)
    own.start()
    for d in range(1, seq):
        mix(d).start()
    for d in order:
        block = lax.rem(s + d, seq)
        for u in range(1, tensor):
            reduce(d, u).wait_recv()
        for e in range(experts):
            value = part_ref[e, block, :, columns(t)].astype(jnp.float32)
            for u in range(1, tensor):
                value += arrived[u - 1, d, e].astype(jnp.float32)
            summed[d, e] = value.astype(jnp.bfloat16)
        if d:
            give(d).start()
    total[...] = cot_ref[...].astype(jnp.float32)
    for d in [0] + list(range(1, seq)):
        block = lax.rem(s - d + seq, seq)
        if d:
            give(d).wait_recv()
        held = back if d else summed
        term = total[...]
        for e in range(experts):
            term += jnp.dot(
                pick_ref[block, e], held[d, e], preferred_element_type=jnp.float32
            )
        total[...] = term
    token_out[t] = total[...].astype(jnp.bfloat16)
    token(1).start()
    token(0).start()
    token(1).wait_recv()
    token(2).start()
    for d in range(seq):
        for u in range(1, tensor):
            reduce(d, u).wait_send()
        if d:
            give(d).wait_send()
            mix(d).wait()
    own.wait()
    token(0).wait()
    token(1).wait_send()
    token(2).wait()


def exchange_kernel(
    seq, tensor, state_ref, token_ref, state_out, token_out, send_sem, recv_sem, own_sem
):
    s = lax.axis_index("sp")
    greet(seq, tensor, s, ())

    def copy(d, which):
        to = lax.rem(s + d, seq)
        if which == 0:
            source, target = state_ref.at[jnp.where(to > s, 0, 1)], state_out.at[s]
        else:
            source, target = token_ref.at[to], token_out.at[s]
        return remote(source, target, send_sem.at[which, d], recv_sem.at[which, d], {"sp": to})

    own = (
        pltpu.make_async_copy(state_ref.at[0], state_out.at[s], own_sem.at[0]),
        pltpu.make_async_copy(token_ref.at[s], token_out.at[s], own_sem.at[1]),
    )
    for which in range(2):
        for d in range(1, seq):
            copy(d, which).start()
    for piece in own:
        piece.start()
    for which in range(2):
        for d in range(1, seq):
            copy(d, which).wait()
    for piece in own:
        piece.wait()


def call(kernel, outs, in_spaces, out_spaces, scratch, number):
    return pl.pallas_call(
        kernel,
        out_shape=outs,
        in_specs=[pl.BlockSpec(memory_space=space) for space in in_spaces],
        out_specs=[pl.BlockSpec(memory_space=space) for space in out_spaces],
        scratch_shapes=scratch,
        compiler_params=pltpu.CompilerParams(collective_id=number, has_side_effects=True),
    )


def running_sum(value):
    row = jnp.arange(value.shape[0], dtype=jnp.int32)
    mask = (row[:, None] >= row[None, :]).astype(jnp.float32)
    return jnp.tensordot(mask, value, 1, precision=lax.Precision.HIGHEST)


def tail_sum(value):
    row = jnp.arange(value.shape[0], dtype=jnp.int32)
    mask = (row[:, None] <= row[None, :]).astype(jnp.float32)
    return jnp.tensordot(mask, value, 1, precision=lax.Precision.HIGHEST)


def local_parts(query_f, key_f, grad_f, pair, decays):
    highest = lax.Precision.HIGH
    sigma = query_f.shape[2] ** (-0.5)
    length = query_f.shape[0]
    cum = running_sum(decays)
    total = cum[-1]
    middle = 0.5 * total
    rise = jnp.exp(cum - middle)
    fall = jnp.exp(middle - cum)
    position = jnp.arange(length, dtype=jnp.int32)
    lower = (position[:, None] >= position[None, :])[None]
    score_fwd = (
        jnp.where(
            lower, jnp.einsum("thc,shc->hts", query_f * rise, key_f * fall, precision=highest), 0.0
        )
        * sigma
    )
    score_bwd = (
        jnp.where(
            lower, 0.0, jnp.einsum("thc,shc->hts", query_f * fall, key_f * rise, precision=highest)
        )
        * sigma
    )
    pair_fwd = jnp.where(lower, pair, 0.0)
    pair_bwd = jnp.where(lower, 0.0, pair)
    query_fwd = sigma * rise * jnp.einsum("hts,shc->thc", pair_fwd, key_f * fall, precision=highest)
    query_bwd = sigma * fall * jnp.einsum("hts,shc->thc", pair_bwd, key_f * rise, precision=highest)
    key_fwd = sigma * fall * jnp.einsum("hts,thc->shc", pair_fwd, query_f * rise, precision=highest)
    key_bwd = sigma * rise * jnp.einsum("hts,thc->shc", pair_bwd, query_f * fall, precision=highest)
    value_grad = jnp.einsum("hts,thv->shv", score_fwd + score_bwd, grad_f, precision=highest)
    return (query_fwd, query_bwd, key_fwd, key_bwd, value_grad, cum, total)


def state_terms(query_f, key_f, value_f, grad_f, cum, total):
    highest = lax.Precision.HIGH
    head_part = jnp.exp(cum)
    tail = jnp.exp(total - cum)
    kv_fwd = jnp.einsum("shc,shv->hcv", key_f * tail, value_f, precision=highest)
    qo_bwd = jnp.einsum("thc,thv->hcv", query_f * tail, grad_f, precision=highest)
    qo_fwd = jnp.einsum("thc,thv->hcv", query_f * head_part, grad_f, precision=highest)
    kv_bwd = jnp.einsum("shc,shv->hcv", key_f * head_part, value_f, precision=highest)
    return (jnp.exp(total), kv_fwd, qo_bwd, qo_fwd, kv_bwd)


def carried(parts, states, query_f, key_f, value_f, grad_f):
    highest = lax.Precision.HIGH
    sigma = query_f.shape[2] ** (-0.5)
    query_fwd, query_bwd, key_fwd, key_bwd, value_grad, cum, total = parts
    kv_low, qo_low, qo_high, kv_high = states
    head_part = jnp.exp(cum)
    tail = jnp.exp(total - cum)
    query_fwd = query_fwd + sigma * head_part * jnp.einsum(
        "thv,hcv->thc", grad_f, kv_low, precision=highest
    )
    query_bwd = query_bwd + sigma * tail * jnp.einsum(
        "thv,hcv->thc", grad_f, kv_high, precision=highest
    )
    key_fwd = key_fwd + sigma * tail * jnp.einsum(
        "shv,hcv->shc", value_f, qo_high, precision=highest
    )
    key_bwd = key_bwd + sigma * head_part * jnp.einsum(
        "shv,hcv->shc", value_f, qo_low, precision=highest
    )
    value_grad = value_grad + sigma * (
        jnp.einsum("shc,hcv->shv", key_f * tail, qo_high, precision=highest)
        + jnp.einsum("shc,hcv->shv", key_f * head_part, qo_low, precision=highest)
    )
    grad_cum = query_f * (query_fwd - query_bwd) - key_f * (key_fwd - key_bwd)
    return (query_fwd + query_bwd, key_fwd + key_bwd, value_grad, grad_cum)


def body(
    queries,
    key_vectors,
    values_in,
    log_decay,
    mixed_heads,
    out_proj,
    layer_input,
    cotangent,
    routes,
    route_weight,
    gate_weight,
    up_weight,
    down_weight,
):
    tokens, top = routes.shape
    seq = lax.axis_size("sp")
    tensor = lax.axis_size("tp")
    s = lax.axis_index("sp")
    experts = gate_weight.shape[0]
    all_experts = experts * seq
    capacity = 2 * tokens * top // all_experts
    model = cotangent.shape[1]
    width = model // tensor
    column = lax.axis_index("tp") * width
    bf16, f32 = jnp.bfloat16, jnp.float32
    dma = pltpu.SemaphoreType.DMA

    heads = queries.shape[1] // DK
    query_f = queries.reshape(tokens, heads, DK).astype(f32)
    key_f = key_vectors.reshape(tokens, heads, DK).astype(f32)
    value_f = values_in.reshape(tokens, heads, DV).astype(f32)
    decays = log_decay.reshape(tokens, heads, DK)
    cum = running_sum(decays)
    total = cum[-1]
    head_part = jnp.exp(cum)
    tail = jnp.exp(total - cum)
    high = lax.Precision.HIGH
    kv_fwd = jnp.einsum("shc,shv->hcv", key_f * tail, value_f, precision=high)
    kv_bwd = jnp.einsum("shc,shv->hcv", key_f * head_part, value_f, precision=high)
    kv_send = jnp.stack([kv_fwd, kv_bwd]).astype(bf16)

    flat_route = routes.reshape(-1)
    onehot = flat_route[:, None] == jnp.arange(all_experts, dtype=jnp.int32)[None, :]
    pair_id = jnp.arange(tokens * top, dtype=jnp.int32)
    before = (pair_id[:, None] > pair_id[None, :]).astype(bf16)
    counts = jnp.dot(before, onehot.astype(bf16), preferred_element_type=f32)
    rank = jnp.sum(jnp.where(onehot, counts, 0.0), axis=1).astype(jnp.int32)
    slot = (flat_route * capacity + rank).reshape(tokens, top)
    slot_id = jnp.arange(all_experts * capacity, dtype=jnp.int32)
    match = slot_id[:, None, None] == slot[None, :, :]
    chosen = jnp.any(match, axis=2).astype(bf16)
    slot_weight = jnp.sum(jnp.where(match, route_weight[None], 0.0), axis=(1, 2))
    pick = (
        jnp.any(
            slot_id.reshape(seq, experts, 1, capacity, 1) == slot[None, None, :, None, :], axis=4
        )
    ).astype(bf16)
    own_input = lax.dynamic_slice_in_dim(layer_input, column, width, 1)
    own_cot = lax.dynamic_slice_in_dim(cotangent, column, width, 1)
    block_shape = (seq, experts, capacity, width)
    rows_send = jnp.dot(chosen, own_input, preferred_element_type=f32).astype(bf16)
    cot_send = (
        slot_weight[:, None] * jnp.dot(chosen, own_cot, preferred_element_type=f32)
    ).astype(bf16)

    expert_shape = jax.ShapeDtypeStruct((experts, seq, capacity, model), bf16)
    expert_rows, weighted, total_all, kv_all = call(
        functools.partial(dispatch_kernel, seq, tensor, width),
        (
            expert_shape,
            expert_shape,
            jax.ShapeDtypeStruct((seq, heads, DK), f32),
            jax.ShapeDtypeStruct((seq, heads, DK, DV), bf16),
        ),
        (VMEM, VMEM, VMEM, VMEM),
        (ANY, ANY, VMEM, VMEM),
        [
            dma((2, seq)),
            dma((2, seq)),
            dma((3, 2, seq)),
            dma((3, 2, seq)),
            dma((2, seq)),
            dma((2, seq)),
            dma((4,)),
        ],
        0,
    )(rows_send.reshape(block_shape), cot_send.reshape(block_shape), total, kv_send)
    expert_rows = expert_rows.reshape(experts, seq * capacity, model)
    weighted = weighted.reshape(experts, seq * capacity, model)

    pre_gate = jnp.einsum("erd,edf->erf", expert_rows, gate_weight, preferred_element_type=f32)
    pre_up = jnp.einsum("erd,edf->erf", expert_rows, up_weight, preferred_element_type=f32)
    d_act = jnp.einsum("erd,efd->erf", weighted, down_weight, preferred_element_type=f32)
    sigmoid_gate = jax.nn.sigmoid(pre_gate)
    silu_gate = pre_gate * sigmoid_gate
    act = (silu_gate * pre_up).astype(bf16)
    d_gate = (d_act * pre_up * sigmoid_gate * (1.0 + pre_gate * (1.0 - sigmoid_gate))).astype(bf16)
    d_up = (d_act * silu_gate).astype(bf16)
    partial_value = (
        jnp.einsum("erf,edf->erd", d_gate, gate_weight, preferred_element_type=f32)
        + jnp.einsum("erf,edf->erd", d_up, up_weight, preferred_element_type=f32)
    ).astype(bf16)
    grad_gate, grad_up, grad_down = (
        jnp.einsum("erd,erf->edf", expert_rows, d_gate, preferred_element_type=f32),
        jnp.einsum("erd,erf->edf", expert_rows, d_up, preferred_element_type=f32),
        jnp.einsum("erf,erd->efd", act, weighted, preferred_element_type=f32),
    )

    token_parts, mixed_all = call(
        functools.partial(return_kernel, seq, tensor, width),
        (
            jax.ShapeDtypeStruct((tensor, tokens, width), bf16),
            jax.ShapeDtypeStruct((seq,) + mixed_heads.shape, bf16),
        ),
        (VMEM, VMEM, VMEM, VMEM),
        (VMEM, ANY),
        [
            pltpu.VMEM((tensor - 1,) + block_shape, bf16),
            pltpu.VMEM(block_shape, bf16),
            pltpu.VMEM(block_shape, bf16),
            pltpu.VMEM((tokens, width), f32),
            dma((tensor - 1, seq)),
            dma((tensor - 1, seq)),
            dma((seq,)),
            dma((seq,)),
            dma((seq,)),
            dma((seq,)),
            dma((3,)),
            dma((3,)),
            dma,
        ],
        1,
    )(
        partial_value.reshape(experts, seq, capacity, model),
        own_cot,
        pick,
        mixed_heads,
    )
    token_grad = jnp.transpose(token_parts, (1, 0, 2)).reshape(tokens, model)
    head_grad = lax.dot_general(
        token_grad, out_proj, (((1,), (1,)), ((), ())), preferred_element_type=f32
    )
    grad_f = head_grad.reshape(tokens, heads, DV)
    qo_bwd = jnp.einsum("thc,thv->hcv", query_f * tail, grad_f, precision=high)
    qo_fwd = jnp.einsum("thc,thv->hcv", query_f * head_part, grad_f, precision=high)
    qo_send = jnp.stack([qo_bwd, qo_fwd]).astype(bf16)
    share = model // seq
    token_send = jnp.transpose(token_grad.reshape(tokens, seq, share), (1, 0, 2))
    qo_all, token_all = call(
        functools.partial(exchange_kernel, seq, tensor),
        (
            jax.ShapeDtypeStruct((seq, heads, DK, DV), bf16),
            jax.ShapeDtypeStruct((seq, tokens, share), bf16),
        ),
        (VMEM, VMEM),
        (VMEM, VMEM),
        [dma((2, seq)), dma((2, seq)), dma((2,))],
        2,
    )(qo_send, token_send)
    grad_proj = lax.dot_general(
        token_all, mixed_all, (((0, 1), (0, 1)), ((), ())), preferred_element_type=f32
    )

    pair = jnp.einsum("thv,shv->hts", grad_f, value_f, precision=high)
    parts = local_parts(query_f, key_f, grad_f, pair, decays)
    block = jnp.arange(seq, dtype=jnp.int32)
    low_span = ((block[None, :] > block[:, None]) & (block[None, :] < s)).astype(f32)
    high_span = ((block[None, :] < block[:, None]) & (block[None, :] > s)).astype(f32)

    def carry(span, mask):
        logs = jnp.sum(span[:, :, None, None] * total_all[None], axis=1)
        return jnp.where(mask[:, None, None], jnp.exp(logs), 0.0)[..., None]

    low_scale = carry(low_span, block < s)
    high_scale = carry(high_span, block > s)
    kv_low = jnp.sum(low_scale * kv_all.astype(f32), axis=0)
    kv_high = jnp.sum(high_scale * kv_all.astype(f32), axis=0)
    qo_low = jnp.sum(low_scale * qo_all.astype(f32), axis=0)
    qo_high = jnp.sum(high_scale * qo_all.astype(f32), axis=0)
    query_grad, key_grad, value_grad, grad_cum = carried(
        parts, (kv_low, qo_low, qo_high, kv_high), query_f, key_f, value_f, grad_f
    )
    decay_all = jnp.exp(total)[..., None]
    beyond = DK ** (-0.5) * jnp.sum(
        (decay_all * kv_low + kv_fwd) * qo_high + (decay_all * qo_low + qo_bwd) * kv_high, axis=2
    )
    grad_decay = tail_sum(grad_cum) + beyond[None]
    return (
        grad_gate,
        grad_up,
        grad_down,
        grad_proj,
        query_grad.reshape(tokens, heads * DK),
        key_grad.reshape(tokens, heads * DK),
        value_grad.reshape(tokens, heads * DV),
        grad_decay.reshape(tokens, heads * DK),
    )


def solution(mesh):
    return jax.shard_map(
        body,
        mesh=mesh,
        in_specs=(
            P("sp", "tp"),
            P("sp", "tp"),
            P("sp", "tp"),
            P("sp", "tp"),
            P("sp", "tp"),
            P("tp", None),
            P("sp", None),
            P("sp", None),
            P("sp", None),
            P("sp", None),
            P("sp", None, "tp"),
            P("sp", None, "tp"),
            P("sp", "tp", None),
        ),
        out_specs=(
            P("sp", None, "tp"),
            P("sp", None, "tp"),
            P("sp", "tp", None),
            P("sp", "tp"),
            P("sp", "tp"),
            P("sp", "tp"),
            P("sp", "tp"),
            P("sp", "tp"),
        ),
        check_vma=False,
    )
```

time: 446 us -> 246 us (0.55)
  waiting for transfers between devices: 203 us -> 0 us
  Pallas kernels: 0 us -> 181 us
  blocking collectives: 106 us -> 0 us
  local copies, waits for them, and re-layouts: 38 us -> 15.2 us
  other arithmetic: 26.8 us -> 7.53 us
  between operations: 16.2 us -> 1.32 us
  matrix products: 47.9 us -> 37.2 us
  starting transfers between devices: 6.03 us -> 0 us
    pallas_call x0 -> x3, Pallas kernels: none -> 181 us  [the longest x1 74.1 us: body(): call(functools.partial(return_kernel, seq, tensor, width), (jax.ShapeDtyp...]
    all_gather x6 -> x0, waiting for transfers between devices: 98.4 us -> none  [the longest x4 85.9 us: carried_in(): pieces = jax.tree.map(lambda part: lax.all_gather(part, axis), value)]
    reduce_scatter x2 -> x0, waiting for transfers between devices: 80.8 us -> none  [the longest x1 47.3 us: body(): lax.psum_scatter(lax.dot_general(token_grad, mixed_heads, (((0,), (0,)),...]
    all_to_all x3 -> x0, blocking collectives: 60.3 us -> none  [the longest x1 27.3 us: body(): lax.all_to_all(input_part.reshape(all_experts, capacity, part_width), 'sp...]
    all_gather x3 -> x0, blocking collectives: 45.5 us -> none  [the longest x2 36.8 us: carried_in(): pieces = jax.tree.map(lambda part: lax.all_gather(part, axis), value)]
    all_to_all x1 -> x0, waiting for transfers between devices: 24 us -> none  [send_back(): lax.all_to_all(row_grad, 'sp', split_axis=1, concat_axis=0, tiled=True)]
    select_n x24 -> x2, other arithmetic: 16.5 us -> 0.16 us  [carry(): return jnp.where(mask[:, None, None], jnp.exp(logs), 0.0)[..., None]]
    rev x6 -> x0, local copies, waits for them, and re-layouts: 9.54 us -> none  [the longest x4 6.24 us: carried_in(): pieces = jax.tree.map(lambda part: part[::-1], pieces)]
  transfers between devices with their start and end apart: 9 -> 0, of which waited for: 6 -> 0; matrix products, arithmetic and copies ran while one was open for 21% -> 0% of each run, Pallas kernels for 0% -> 0%
where the time goes in v1:
time: 246 us; the launch traced here: 242 us
  Pallas kernels  181 us (74%)
  matrix products  37.2 us (15%)
  local copies, waits for them, and re-layouts  15.2 us (6%)
  other arithmetic  7.53 us (3%)
    pallas_call x1, Pallas kernels, body(): call(functools.partial(return_kernel, seq, tensor, width), (jax.ShapeDtyp...  74.1 us
    pallas_call x1, Pallas kernels, body(): call(functools.partial(dispatch_kernel, seq, tensor, width), (expert_shap...  60.1 us
    pallas_call x1, Pallas kernels, body(): call(functools.partial(exchange_kernel, seq, tensor), (jax.ShapeDtypeStru...  46.8 us

profile of v1, /device:TPU:0, one launch (start us, length us, event | category | flops | bytes accessed | tf_op | source)
XLA Modules:
  0.0 242.3 jit_solution(2020790579900774821)
XLA Ops:
  0.7 1.3 fusion.42
  2.0 1.0 convert_bitcast_fusion
  3.0 1.3 fusion.40
  4.4 0.4 fusion.23
  5.0 0.7 pad_maximum_fusion.state_ref
  5.8 0.9 constant_dynamic-slice_fusion.cot_ref
  7.8 1.3 multiply_convert_fusion
  9.1 2.2 convolution_convert_fusion
  11.4 60.1 %shard_map.188 = (bf16[2,8,48,2048]{3,2,1,0:T(8,128)(2,1)}, bf16[2,8,48,2048]{3,2,1,0:T(8,128)(2,1)}, f32[8,2,128]{2,1,0:T(2,128)}, bf16[8,2,128,256]{3,2,1,0:T(8,128)(2,1)}) custom-call(bf16[8,2,48,512]{3,2,1,0:T(8,128)(2,1)} %bitcast.192, bf16[8,2,48,512]{3,2,1,0:T(8,128)(2,1)} %bitcast.195, f32[2,128]{1,0:T(2,128)} %bitcast.200, ...), custom_call_target="tpu_custom_call" | custom-call | tf_op jit(solution)/shard_map/pallas_call | solution.py:453
  71.5 3.7 %fusion.87 = f32[2,384,256]{2,1,0:T(8,128)S(1)} fusion(bf16[2,384,2048]{2,1,0:T(8,128)(2,1)} %bitcast.180, bf16[2,2048,256]{2,1,0:T(8,128)(2,1)} %param.24), kind=kOutput, calls=%fused_computation.157 | convolution fusion | flops 805306368 | bytes 6029312 | tf_op jit(solution)/shard_map/erd,edf->erf/dot_general | solution.py:478
  75.2 1.0 fusion.88
  76.3 1.4 copy-done.7
  77.7 0.6 copy-done.27
  78.3 1.2 multiply_convert_fusion.2
  79.6 1.0 fusion.91
  80.6 0.8 copy-done.3
  81.4 2.7 %add_convert_fusion = bf16[2,384,2048]{2,1,0:T(8,128)(2,1)} fusion(f32[2,384,2048]{2,1,0:T(8,128)S(1)} %fusion.91, bf16[2,384,256]{2,1,0:T(8,128)(2,1)S(1)} %get-tuple-element.32, bf16[2,2048,256]{2,1,0:T(8,128)(2,1)S(1)} %copy-done.3), kind=kOutput, calls=%fused_computation | convolution fusion | flops 808452096 | bytes 11927552 | tf_op jit(solution)/shard_map/erf,edf->erd/dot_general | solution.py:487
  84.4 1.2 copy.120.pick_ref
  85.7 74.1 %shard_map.189 = (bf16[4,192,512]{2,1,0:T(8,128)(2,1)}, bf16[8,192,512]{2,1,0:T(8,128)(2,1)}) custom-call(bf16[2,8,48,2048]{3,2,1,0:T(8,128)(2,1)} %bitcast.184, bf16[192,512]{1,0:T(8,128)(2,1)} %copy-done.20, bf16[8,2,192,48]{3,2,1,0:T(8,128)(2,1)} %copy.120.pick_ref, bf16[192,512]{1,0:T(8,128)(2,1)} %mixed_ref.1), custom_call_target="tpu_custom_call" | custom-call | tf_op jit(solution)/shard_map/pallas_call | solution.py:495
  159.8 1.7 copy.121
  161.6 1.5 reshape.232
  163.1 2.7 %fusion.92 = f32[192,2,256]{2,0,1:T(8,128)S(1)} fusion(bf16[192,2048,1]{1,0,2:T(8,128)(2,1)} %reshape.232, bf16[2,256,2048]{2,1,0:T(8,128)(2,1)} %bitcast.194), kind=kOutput, calls=%fused_computation.162 | convolution fusion | flops 402653184 | bytes 3276800 | tf_op jit(solution)/shard_map/dot_general | solution.py:526
  165.8 0.4 fusion.32
  166.2 0.4 fusion.24
  166.7 0.7 pad_maximum_fusion.1.state_ref
  167.4 2.4 reshape_reshape.3
  169.8 2.2 copy.219
  172.0 46.8 %shard_map.190 = (bf16[8,2,128,256]{3,2,1,0:T(8,128)(2,1)}, bf16[8,192,256]{2,1,0:T(8,128)(2,1)}) custom-call(bf16[2,2,128,256]{3,2,1,0:T(8,128)(2,1)} %pad_maximum_fusion.1.state_ref, bf16[8,192,256]{2,1,0:T(8,128)(2,1)} %bitcast.193), custom_call_target="tpu_custom_call" | custom-call | tf_op jit(solution)/shard_map/pallas_call | solution.py:535
  219.1 2.4 fusion.1
  222.2 0.6 fusion.13
  223.0 0.6 fusion.16
  223.9 0.3 fusion.19
  224.2 0.3 fusion.18
  224.6 0.3 fusion.22
  224.9 0.3 fusion.21
  225.3 0.3 fusion.10
  225.6 0.7 copy.220
  226.6 0.4 convolution_select_fusion
  227.0 0.4 fusion.5
  227.4 0.6 fusion.93
  228.0 0.4 fusion.8
  228.3 0.8 copy.155
  229.1 0.7 copy_bitcast_fusion.2
  229.8 0.7 copy_bitcast_fusion.3
  230.5 1.4 convolution_bitcast_fusion
  232.0 3.4 %fusion.27 = f32[2,256,2048]{2,1,0:T(8,128)} fusion(bf16[2,384,2048]{2,1,0:T(8,128)(2,1)S(1)} %bitcast.191, f32[2,384,256]{2,1,0:T(8,128)S(1)} %copy-done.10, f32[2,384,256]{2,1,0:T(8,128)S(1)} %copy-done.12), kind=kOutput, calls=%fused_computation.59 | convolution fusion | flops 806486016 | bytes 8912896 | tf_op jit(solution)/shard_map/erf,erd->efd/dot_general | solution.py:492
  235.3 3.5 %fusion.90 = f32[2,2048,256]{2,1,0:T(8,128)} fusion(bf16[2,384,2048]{2,1,0:T(8,128)(2,1)S(1)} %bitcast.182, bf16[2,384,256]{2,1,0:T(8,128)(2,1)S(1)} %copy-done.18), kind=kOutput, calls=%fused_computation.160 | convolution fusion | flops 805306368 | bytes 7733248 | tf_op jit(solution)/shard_map/erd,erf->edf/dot_general | solution.py:491
  238.8 3.5 %fusion.89 = f32[2,2048,256]{2,1,0:T(8,128)} fusion(bf16[2,384,2048]{2,1,0:T(8,128)(2,1)S(1)} %bitcast.183, bf16[2,384,256]{2,1,0:T(8,128)(2,1)S(1)} %copy-done.16), kind=kOutput, calls=%fused_computation.159 | convolution fusion | flops 805306368 | bytes 7733248 | tf_op jit(solution)/shard_map/erd,erf->edf/dot_general | solution.py:490
  (84 shorter events, 3.6 us)
Async XLA Ops:
  0.6 74.5 %copy-start = (bf16[2,2048,256]{2,1,0:T(8,128)(2,1)S(1)}, bf16[2,2048,256]{2,1,0:T(8,128)(2,1)}, u32[]{:S(2)}) copy-start(bf16[2,2048,256]{2,1,0:T(8,128)(2,1)} %param.23) | copy-start | bytes 6291460
  0.6 3.7 %copy-start.5 = (bf16[192,512]{1,0:T(8,128)(2,1)S(1)}, bf16[192,512]{1,0:T(8,128)(2,1)}, u32[]{:S(2)}) copy-start(bf16[192,512]{1,0:T(8,128)(2,1)} %param.15) | copy-start | bytes 589828
  0.7 6.0 %copy-start.24 = (s32[192,2]{0,1:T(2,128)S(1)}, s32[192,2]{0,1:T(2,128)}, u32[]{:S(2)}) copy-start(s32[192,2]{0,1:T(2,128)} %param.21) | copy-start | bytes 4612
  2.0 5.6 %copy-start.22 = (f32[1,2,128]{2,0,1:T(1,128)}, f32[1,2,128]{2,0,1:T(1,128)S(1)}, u32[]{:S(2)}) copy-start(f32[1,2,128]{2,0,1:T(1,128)S(1)} %slice.5) | copy-start | bytes 3076
  2.0 5.6 %copy-start.26 = (f32[192,2]{0,1:T(2,128)S(1)}, f32[192,2]{0,1:T(2,128)}, u32[]{:S(2)}) copy-start(f32[192,2]{0,1:T(2,128)} %param.22) | copy-start | bytes 4612
  4.3 0.7 copy-start.13
  6.7 64.8 %copy-start.20 = (bf16[192,512]{1,0:T(8,128)(2,1)}, bf16[192,512]{1,0:T(8,128)(2,1)S(1)}, u32[]{:S(2)}) copy-start(bf16[192,512]{1,0:T(8,128)(2,1)S(1)} %constant_dynamic-slice_fusion.cot_ref) | copy-start | bytes 589828
  71.5 3.7 %copy-start.1 = (bf16[2,8,48,2048]{3,2,1,0:T(8,128)(2,1)S(1)}, bf16[2,8,48,2048]{3,2,1,0:T(8,128)(2,1)}, u32[]{:S(2)}) copy-start(bf16[2,8,48,2048]{3,2,1,0:T(8,128)(2,1)} %get-tuple-element.16) | copy-start | bytes 9437188
  75.2 1.1 copy-start.9
  75.2 2.5 %copy-start.7 = (bf16[2,8,48,2048]{3,2,1,0:T(8,128)(2,1)S(1)}, bf16[2,8,48,2048]{3,2,1,0:T(8,128)(2,1)}, u32[]{:S(2)}) copy-start(bf16[2,8,48,2048]{3,2,1,0:T(8,128)(2,1)} %get-tuple-element.17) | copy-start | bytes 9437188
  75.2 3.1 %copy-start.27 = (bf16[2,256,2048]{2,1,0:T(8,128)(2,1)S(1)}, bf16[2,256,2048]{2,1,0:T(8,128)(2,1)}, u32[]{:S(2)}) copy-start(bf16[2,256,2048]{2,1,0:T(8,128)(2,1)} %param.25) | copy-start | bytes 6291460
  76.3 3.3 %copy-start.11 = (f32[2,384,256]{2,1,0:T(8,128)}, f32[2,384,256]{2,1,0:T(8,128)S(1)}, u32[]{:S(2)}) copy-start(f32[2,384,256]{2,1,0:T(8,128)S(1)} %fusion.88) | copy-start | bytes 2359300
  79.5 1.1 copy-start.15
  79.5 1.1 copy-start.17
  79.5 1.9 copy-start.3
  161.6 1.5 copy-start.4
  161.6 4.2 %copy-start.23 = (f32[1,2,128]{2,0,1:T(1,128)S(1)}, f32[1,2,128]{2,0,1:T(1,128)}, u32[]{:S(2)}) copy-start(f32[1,2,128]{2,0,1:T(1,128)} %copy-done.22) | copy-start | bytes 3076
  167.4 51.4 %copy-start.25 = (f32[8,2,128]{2,1,0:T(2,128)S(1)}, f32[8,2,128]{2,1,0:T(2,128)}, u32[]{:S(2)}) copy-start(f32[8,2,128]{2,1,0:T(2,128)} %get-tuple-element.21) | copy-start | bytes 24580
  218.8 2.8 %copy-start.14 = (f32[2,128,256]{2,1,0:T(8,128)S(1)}, f32[2,128,256]{2,1,0:T(8,128)}, u32[]{:S(2)}) copy-start(f32[2,128,256]{2,1,0:T(8,128)} %copy-done.13) | copy-start | bytes 786436
  219.1 2.7 %copy-start.6 = (bf16[192,512]{1,0:T(8,128)(2,1)S(1)}, bf16[192,512]{1,0:T(8,128)(2,1)}, u32[]{:S(2)}) copy-start(bf16[192,512]{1,0:T(8,128)(2,1)} %param.15) | copy-start | bytes 589828
  227.4 3.2 %copy-start.21 = (bf16[8,192,256]{2,1,0:T(8,128)(2,1)S(1)}, bf16[8,192,256]{2,1,0:T(8,128)(2,1)}, u32[]{:S(2)}) copy-start(bf16[8,192,256]{2,1,0:T(8,128)(2,1)} %get-tuple-element.19) | copy-start | bytes 2359300
  228.0 2.6 %copy-start.19 = (bf16[8,192,512]{2,1,0:T(8,128)(2,1)S(1)}, bf16[8,192,512]{2,1,0:T(8,128)(2,1)}, u32[]{:S(2)}) copy-start(bf16[8,192,512]{2,1,0:T(8,128)(2,1)} %get-tuple-element.20) | copy-start | bytes 4718596
  228.3 3.6 %copy-start.12 = (f32[2,384,256]{2,1,0:T(8,128)S(1)}, f32[2,384,256]{2,1,0:T(8,128)}, u32[]{:S(2)}) copy-start(f32[2,384,256]{2,1,0:T(8,128)} %copy-done.11) | copy-start | bytes 2359300
  229.1 2.8 %copy-start.8 = (bf16[2,8,48,2048]{3,2,1,0:T(8,128)(2,1)S(1)}, bf16[2,8,48,2048]{3,2,1,0:T(8,128)(2,1)}, u32[]{:S(2)}) copy-start(bf16[2,8,48,2048]{3,2,1,0:T(8,128)(2,1)} %get-tuple-element.17) | copy-start | bytes 9437188
  229.1 2.8 %copy-start.10 = (f32[2,384,256]{2,1,0:T(8,128)S(1)}, f32[2,384,256]{2,1,0:T(8,128)}, u32[]{:S(2)}) copy-start(f32[2,384,256]{2,1,0:T(8,128)} %copy-done.9) | copy-start | bytes 2359300
  231.9 3.4 %copy-start.2 = (bf16[2,8,48,2048]{3,2,1,0:T(8,128)(2,1)S(1)}, bf16[2,8,48,2048]{3,2,1,0:T(8,128)(2,1)}, u32[]{:S(2)}) copy-start(bf16[2,8,48,2048]{3,2,1,0:T(8,128)(2,1)} %get-tuple-element.16) | copy-start | bytes 9437188
  231.9 3.4 %copy-start.18 = (bf16[2,384,256]{2,1,0:T(8,128)(2,1)S(1)}, bf16[2,384,256]{2,1,0:T(8,128)(2,1)}, u32[]{:S(2)}) copy-start(bf16[2,384,256]{2,1,0:T(8,128)(2,1)} %copy-done.17) | copy-start | bytes 1179652
  235.3 3.5 %copy-start.16 = (bf16[2,384,256]{2,1,0:T(8,128)(2,1)S(1)}, bf16[2,384,256]{2,1,0:T(8,128)(2,1)}, u32[]{:S(2)}) copy-start(bf16[2,384,256]{2,1,0:T(8,128)(2,1)} %copy-done.15) | copy-start | bytes 1179652

commit v2 on v1

--- a/solution.py
+++ b/solution.py
@@ -45,6 +45,40 @@
     beside = t + 1 - 2 * lax.rem(t, 2)
     across = lax.rem(t + tensor // 2, tensor)
     return t, beside, across
+
+
+class Relay:
+    def __init__(self, seq, s, source, out, send_sem, recv_sem):
+        self.half = seq // 2
+        other = s + 1 - 2 * lax.rem(s, 2)
+
+        def direct(j):
+            to = lax.rem(s + 2 * j, seq)
+            return remote(source(to), out.at[s], send_sem(j), recv_sem(j), {"sp": to})
+
+        def onward(j):
+            block = lax.rem(s - 2 * j + seq, seq)
+            place = self.half + j
+            held = out.at[block] if j else source(other)
+            return remote(held, out.at[block], send_sem(place), recv_sem(place), {"sp": other})
+
+        self.direct, self.onward = direct, onward
+
+    def start(self):
+        for j in range(1, self.half):
+            self.direct(j).start()
+        self.onward(0).start()
+
+    def forward(self):
+        for j in range(1, self.half):
+            self.direct(j).wait_recv()
+            self.onward(j).start()
+
+    def finish(self):
+        for j in range(self.half):
+            if j:
+                self.direct(j).wait_send()
+            self.onward(j).wait()
 
 
 def dispatch_kernel(
@@ -96,15 +130,20 @@
             {"tp": across if way == 1 else beside},
         )
 
-    def small(d, which):
+    def small(d):
         to = lax.rem(s + d, seq)
-        if which == 0:
-            source, target = total_ref, total_out.at[s]
-        else:
-            source, target = state_ref.at[jnp.where(to > s, 0, 1)], state_out.at[s]
         return remote(
-            source, target, small_send.at[which, d], small_recv.at[which, d], {"sp": to}
-        )
+            total_ref, total_out.at[s], small_send.at[0, d], small_recv.at[0, d], {"sp": to}
+        )
+
+    states = Relay(
+        seq,
+        s,
+        lambda to: state_ref.at[jnp.where(to > s, 0, 1)],
+        state_out,
+        lambda i: small_send.at[1, i],
+        lambda i: small_recv.at[1, i],
+    )
 
     for d in range(1, seq):
         for a in range(2):
@@ -121,8 +160,8 @@
         forward(a, 0, 1).start()
         forward(a, 0, 0).start()
     for d in range(1, seq):
-        small(d, 0).start()
-        small(d, 1).start()
+        small(d).start()
+    states.start()
     lag = 2
     for d in range(1, seq + lag):
         if d < seq:
@@ -134,6 +173,7 @@
             for a in range(2):
                 forward(a, d - lag, 1).wait_recv()
                 forward(a, d - lag, 2).start()
+    states.forward()
     for d in range(seq):
         for a in range(2):
             if d:
@@ -142,8 +182,8 @@
             forward(a, d, 1).wait_send()
             forward(a, d, 2).wait()
         if d:
-            small(d, 0).wait()
-            small(d, 1).wait()
+            small(d).wait()
+    states.finish()
     for copy in own:
         copy.wait()
 
@@ -195,11 +235,14 @@
         to = lax.rem(s + d, seq)
         return remote(summed.at[d], back.at[d], sp_send.at[d], sp_recv.at[d], {"sp": to})
 
-    def mix(d):
-        to = lax.rem(s + d, seq)
-        return remote(
-            mixed_ref, mixed_out.at[s], mix_send.at[d], mix_recv.at[d], {"sp": to}
-        )
+    mix = Relay(
+        seq,
+        s,
+        lambda to: mixed_ref,
+        mixed_out,
+        lambda i: mix_send.at[i],
+        lambda i: mix_recv.at[i],
+    )
 
     def token(way):
         part = across if way == 2 else t
@@ -217,8 +260,7 @@
             reduce(d, u).start()
     own = pltpu.make_async_copy(mixed_ref, mixed_out.at[s], own_sem)
     own.start()
-    for d in range(1, seq):
-        mix(d).start()
+    mix.start()
     for d in order:
         block = lax.rem(s + d, seq)
         for u in range(1, tensor):
@@ -230,6 +272,7 @@
             summed[d, e] = value.astype(jnp.bfloat16)
         if d:
             give(d).start()
+    mix.forward()
     total[...] = cot_ref[...].astype(jnp.float32)
     for d in [0] + list(range(1, seq)):
         block = lax.rem(s - d + seq, seq)
@@ -252,7 +295,7 @@
             reduce(d, u).wait_send()
         if d:
             give(d).wait_send()
-            mix(d).wait()
+    mix.finish()
     own.wait()
     token(0).wait()
     token(1).wait_send()
@@ -265,26 +308,34 @@
     s = lax.axis_index("sp")
     greet(seq, tensor, s, ())
 
-    def copy(d, which):
+    states = Relay(
+        seq,
+        s,
+        lambda to: state_ref.at[jnp.where(to > s, 0, 1)],
+        state_out,
+        lambda i: send_sem.at[0, i],
+        lambda i: recv_sem.at[0, i],
+    )
+
+    def copy(d):
         to = lax.rem(s + d, seq)
-        if which == 0:
-            source, target = state_ref.at[jnp.where(to > s, 0, 1)], state_out.at[s]
-        else:
-            source, target = token_ref.at[to], token_out.at[s]
-        return remote(source, target, send_sem.at[which, d], recv_sem.at[which, d], {"sp": to})
+        return remote(
+            token_ref.at[to], token_out.at[s], send_sem.at[1, d], recv_sem.at[1, d], {"sp": to}
+        )
 
     own = (
         pltpu.make_async_copy(state_ref.at[0], state_out.at[s], own_sem.at[0]),
         pltpu.make_async_copy(token_ref.at[s], token_out.at[s], own_sem.at[1]),
     )
-    for which in range(2):
-        for d in range(1, seq):
-            copy(d, which).start()
+    states.start()
+    for d in range(1, seq):
+        copy(d).start()
     for piece in own:
         piece.start()
-    for which in range(2):
-        for d in range(1, seq):
-            copy(d, which).wait()
+    states.forward()
+    for d in range(1, seq):
+        copy(d).wait()
+    states.finish()
     for piece in own:
         piece.wait()
 

time: 246 us -> 225 us (0.915)
  Pallas kernels: 181 us -> 160 us
    pallas_call x1, Pallas kernels: 46.8 us -> 30.2 us  [body(): call(functools.partial(exchange_kernel, seq, tensor), (jax.ShapeDtypeStru...]
    pallas_call x1, Pallas kernels: 74.1 us -> 67.3 us  [body(): call(functools.partial(return_kernel, seq, tensor, width), (jax.ShapeDtyp...]
where the time goes in v2:
time: 225 us; the launch traced here: 221 us
  Pallas kernels  160 us (71%)
  matrix products  37.3 us (17%)
  local copies, waits for them, and re-layouts  15.2 us (7%)
  other arithmetic  7.53 us (3%)
    pallas_call x1, Pallas kernels, body(): call(functools.partial(return_kernel, seq, tensor, width), (jax.ShapeDtyp...  67.3 us
    pallas_call x1, Pallas kernels, body(): call(functools.partial(dispatch_kernel, seq, tensor, width), (expert_shap...  62.3 us
    pallas_call x1, Pallas kernels, body(): call(functools.partial(exchange_kernel, seq, tensor), (jax.ShapeDtypeStru...  30.2 us
    another operation x2, local copies, waits for them, and re-layouts, body(): token_grad.reshape(tokens, seq, share)  4.53 us

profile of v2, /device:TPU:0, one launch (start us, length us, event | category | flops | bytes accessed | tf_op | source)
XLA Modules:
  0.0 221.0 jit_solution(7162890047081067595)
XLA Ops:
  0.7 1.3 fusion.42
  2.0 1.0 convert_bitcast_fusion
  3.0 1.3 fusion.40
  4.4 0.4 fusion.23
  5.0 0.7 pad_maximum_fusion.state_ref
  5.8 0.9 constant_dynamic-slice_fusion.cot_ref
  7.8 1.3 multiply_convert_fusion
  9.1 2.2 %convolution_convert_fusion = bf16[768,512]{1,0:T(8,128)(2,1)} fusion(pred[768,192]{0,1:T(8,128)(4,1)S(1)} %fusion.9, bf16[192,2048]{1,0:T(8,128)(2,1)} %param.19, s32[]{:T(128)S(6)} %select_n.42), kind=kOutput, calls=%fused_computation.11 | convolution fusion | flops 151388160 | bytes 1130500 | tf_op jit(solution)/shard_map/dot_general | solution.py:498
  11.4 62.3 %shard_map.188 = (bf16[2,8,48,2048]{3,2,1,0:T(8,128)(2,1)}, bf16[2,8,48,2048]{3,2,1,0:T(8,128)(2,1)}, f32[8,2,128]{2,1,0:T(2,128)}, bf16[8,2,128,256]{3,2,1,0:T(8,128)(2,1)}) custom-call(bf16[8,2,48,512]{3,2,1,0:T(8,128)(2,1)} %bitcast.192, bf16[8,2,48,512]{3,2,1,0:T(8,128)(2,1)} %bitcast.195, f32[2,128]{1,0:T(2,128)} %bitcast.200, ...), custom_call_target="tpu_custom_call" | custom-call | tf_op jit(solution)/shard_map/pallas_call | solution.py:504
  73.7 3.7 %fusion.87 = f32[2,384,256]{2,1,0:T(8,128)S(1)} fusion(bf16[2,384,2048]{2,1,0:T(8,128)(2,1)} %bitcast.180, bf16[2,2048,256]{2,1,0:T(8,128)(2,1)} %param.24), kind=kOutput, calls=%fused_computation.157 | convolution fusion | flops 805306368 | bytes 6029312 | tf_op jit(solution)/shard_map/erd,edf->erf/dot_general | solution.py:529
  77.5 1.0 fusion.88
  78.5 1.4 copy-done.7
  79.9 0.6 copy-done.27
  80.5 1.2 multiply_convert_fusion.2
  81.8 1.0 fusion.91
  82.8 0.8 copy-done.3
  83.7 2.7 %add_convert_fusion = bf16[2,384,2048]{2,1,0:T(8,128)(2,1)} fusion(f32[2,384,2048]{2,1,0:T(8,128)S(1)} %fusion.91, bf16[2,384,256]{2,1,0:T(8,128)(2,1)S(1)} %get-tuple-element.32, bf16[2,2048,256]{2,1,0:T(8,128)(2,1)S(1)} %copy-done.3), kind=kOutput, calls=%fused_computation | convolution fusion | flops 808452096 | bytes 11927552 | tf_op jit(solution)/shard_map/erf,edf->erd/dot_general | solution.py:538
  86.7 1.2 copy.120.pick_ref
  87.9 67.3 %shard_map.189 = (bf16[4,192,512]{2,1,0:T(8,128)(2,1)}, bf16[8,192,512]{2,1,0:T(8,128)(2,1)}) custom-call(bf16[2,8,48,2048]{3,2,1,0:T(8,128)(2,1)} %bitcast.184, bf16[192,512]{1,0:T(8,128)(2,1)} %copy-done.20, bf16[8,2,192,48]{3,2,1,0:T(8,128)(2,1)} %copy.120.pick_ref, bf16[192,512]{1,0:T(8,128)(2,1)} %mixed_ref.1), custom_call_target="tpu_custom_call" | custom-call | tf_op jit(solution)/shard_map/pallas_call | solution.py:546
  155.2 1.7 copy.121
  157.0 1.5 reshape.232
  158.4 2.7 %fusion.92 = f32[192,2,256]{2,0,1:T(8,128)S(1)} fusion(bf16[192,2048,1]{1,0,2:T(8,128)(2,1)} %reshape.232, bf16[2,256,2048]{2,1,0:T(8,128)(2,1)} %bitcast.194), kind=kOutput, calls=%fused_computation.162 | convolution fusion | flops 402653184 | bytes 3276800 | tf_op jit(solution)/shard_map/dot_general | solution.py:577
  161.1 0.4 fusion.32
  161.6 0.4 fusion.24
  162.1 0.7 pad_maximum_fusion.1.state_ref
  162.8 2.4 %reshape_reshape.3 = bf16[192,8,256]{2,1,0:T(8,128)(2,1)} reshape(bf16[192,4,512]{2,1,0:T(4,128)(2,1)} %copy-done.4) | data formatting | bytes 1572864 | tf_op jit(solution)/shard_map/reshape;reshape | solution.py:585
  165.1 2.2 copy.219
  167.3 30.2 %shard_map.190 = (bf16[8,2,128,256]{3,2,1,0:T(8,128)(2,1)}, bf16[8,192,256]{2,1,0:T(8,128)(2,1)}) custom-call(bf16[2,2,128,256]{3,2,1,0:T(8,128)(2,1)} %pad_maximum_fusion.1.state_ref, bf16[8,192,256]{2,1,0:T(8,128)(2,1)} %bitcast.193), custom_call_target="tpu_custom_call" | custom-call | tf_op jit(solution)/shard_map/pallas_call | solution.py:586
  197.9 2.4 %fusion.1 = (f32[2,128,256]{2,1,0:T(8,128)S(1)}, f32[2,128,256]{2,1,0:T(8,128)S(1)}, f32[2,128,256]{2,1,0:T(8,128)S(1)}, f32[2,128,256]{2,1,0:T(8,128)S(1)}) fusion(bf16[8,2,128,256]{3,2,1,0:T(8,128)(2,1)} %get-tuple-element.22, f32[8,2,128]{2,1,0:T(2,128)S(1)} %exponential_select_fusion, f32[8,2,128]{2,1,0:T(2,128)S(1)} %exponential_select_fusion.1, ...), kind=kLoop, calls=%fused_computation.6 | loop fusion | flops 4980736 | bytes 3162112 | tf_op jit(solution)/shard_map/reduce_sum | solution.py:614
  200.9 0.6 fusion.13
  201.8 0.6 fusion.16
  202.6 0.3 fusion.19
  203.0 0.3 fusion.18
  203.3 0.3 fusion.22
  203.7 0.3 fusion.21
  204.0 0.3 fusion.10
  204.3 0.7 copy.220
  205.3 0.4 convolution_select_fusion
  205.7 0.4 fusion.5
  206.1 0.6 fusion.93
  206.7 0.4 fusion.8
  207.1 0.8 copy.155
  207.9 0.7 copy_bitcast_fusion.2
  208.6 0.7 copy_bitcast_fusion.3
  209.3 1.4 convolution_bitcast_fusion
  210.7 3.3 %fusion.27 = f32[2,256,2048]{2,1,0:T(8,128)} fusion(bf16[2,384,2048]{2,1,0:T(8,128)(2,1)S(1)} %bitcast.191, f32[2,384,256]{2,1,0:T(8,128)S(1)} %copy-done.10, f32[2,384,256]{2,1,0:T(8,128)S(1)} %copy-done.12), kind=kOutput, calls=%fused_computation.59 | convolution fusion | flops 806486016 | bytes 8912896 | tf_op jit(solution)/shard_map/erf,erd->efd/dot_general | solution.py:543
  214.1 3.5 %fusion.90 = f32[2,2048,256]{2,1,0:T(8,128)} fusion(bf16[2,384,2048]{2,1,0:T(8,128)(2,1)S(1)} %bitcast.182, bf16[2,384,256]{2,1,0:T(8,128)(2,1)S(1)} %copy-done.18), kind=kOutput, calls=%fused_computation.160 | convolution fusion | flops 805306368 | bytes 7733248 | tf_op jit(solution)/shard_map/erd,erf->edf/dot_general | solution.py:542
  217.5 3.5 %fusion.89 = f32[2,2048,256]{2,1,0:T(8,128)} fusion(bf16[2,384,2048]{2,1,0:T(8,128)(2,1)S(1)} %bitcast.183, bf16[2,384,256]{2,1,0:T(8,128)(2,1)S(1)} %copy-done.16), kind=kOutput, calls=%fused_computation.159 | convolution fusion | flops 805306368 | bytes 7733248 | tf_op jit(solution)/shard_map/erd,erf->edf/dot_general | solution.py:541
  (84 shorter events, 3.6 us)
Async XLA Ops:
  0.6 76.8 %copy-start = (bf16[2,2048,256]{2,1,0:T(8,128)(2,1)S(1)}, bf16[2,2048,256]{2,1,0:T(8,128)(2,1)}, u32[]{:S(2)}) copy-start(bf16[2,2048,256]{2,1,0:T(8,128)(2,1)} %param.23) | copy-start | bytes 6291460
  0.6 3.7 %copy-start.5 = (bf16[192,512]{1,0:T(8,128)(2,1)S(1)}, bf16[192,512]{1,0:T(8,128)(2,1)}, u32[]{:S(2)}) copy-start(bf16[192,512]{1,0:T(8,128)(2,1)} %param.15) | copy-start | bytes 589828
  0.7 6.0 %copy-start.24 = (s32[192,2]{0,1:T(2,128)S(1)}, s32[192,2]{0,1:T(2,128)}, u32[]{:S(2)}) copy-start(s32[192,2]{0,1:T(2,128)} %param.21) | copy-start | bytes 4612
  2.0 5.6 %copy-start.22 = (f32[1,2,128]{2,0,1:T(1,128)}, f32[1,2,128]{2,0,1:T(1,128)S(1)}, u32[]{:S(2)}) copy-start(f32[1,2,128]{2,0,1:T(1,128)S(1)} %slice.5) | copy-start | bytes 3076
  2.0 5.6 %copy-start.26 = (f32[192,2]{0,1:T(2,128)S(1)}, f32[192,2]{0,1:T(2,128)}, u32[]{:S(2)}) copy-start(f32[192,2]{0,1:T(2,128)} %param.22) | copy-start | bytes 4612
  4.3 0.7 copy-start.13
  6.7 67.0 %copy-start.20 = (bf16[192,512]{1,0:T(8,128)(2,1)}, bf16[192,512]{1,0:T(8,128)(2,1)S(1)}, u32[]{:S(2)}) copy-start(bf16[192,512]{1,0:T(8,128)(2,1)S(1)} %constant_dynamic-slice_fusion.cot_ref) | copy-start | bytes 589828
  73.7 3.7 %copy-start.1 = (bf16[2,8,48,2048]{3,2,1,0:T(8,128)(2,1)S(1)}, bf16[2,8,48,2048]{3,2,1,0:T(8,128)(2,1)}, u32[]{:S(2)}) copy-start(bf16[2,8,48,2048]{3,2,1,0:T(8,128)(2,1)} %get-tuple-element.16) | copy-start | bytes 9437188
  77.4 1.1 copy-start.9
  77.4 2.5 %copy-start.7 = (bf16[2,8,48,2048]{3,2,1,0:T(8,128)(2,1)S(1)}, bf16[2,8,48,2048]{3,2,1,0:T(8,128)(2,1)}, u32[]{:S(2)}) copy-start(bf16[2,8,48,2048]{3,2,1,0:T(8,128)(2,1)} %get-tuple-element.17) | copy-start | bytes 9437188
  77.4 3.1 %copy-start.27 = (bf16[2,256,2048]{2,1,0:T(8,128)(2,1)S(1)}, bf16[2,256,2048]{2,1,0:T(8,128)(2,1)}, u32[]{:S(2)}) copy-start(bf16[2,256,2048]{2,1,0:T(8,128)(2,1)} %param.25) | copy-start | bytes 6291460
  78.5 3.3 %copy-start.11 = (f32[2,384,256]{2,1,0:T(8,128)}, f32[2,384,256]{2,1,0:T(8,128)S(1)}, u32[]{:S(2)}) copy-start(f32[2,384,256]{2,1,0:T(8,128)S(1)} %fusion.88) | copy-start | bytes 2359300
  81.8 1.1 copy-start.15
  81.8 1.1 copy-start.17
  81.8 1.9 copy-start.3
  156.9 1.5 copy-start.4
  156.9 4.2 %copy-start.23 = (f32[1,2,128]{2,0,1:T(1,128)S(1)}, f32[1,2,128]{2,0,1:T(1,128)}, u32[]{:S(2)}) copy-start(f32[1,2,128]{2,0,1:T(1,128)} %copy-done.22) | copy-start | bytes 3076
  162.8 34.7 %copy-start.25 = (f32[8,2,128]{2,1,0:T(2,128)S(1)}, f32[8,2,128]{2,1,0:T(2,128)}, u32[]{:S(2)}) copy-start(f32[8,2,128]{2,1,0:T(2,128)} %get-tuple-element.21) | copy-start | bytes 24580
  197.5 2.8 %copy-start.14 = (f32[2,128,256]{2,1,0:T(8,128)S(1)}, f32[2,128,256]{2,1,0:T(8,128)}, u32[]{:S(2)}) copy-start(f32[2,128,256]{2,1,0:T(8,128)} %copy-done.13) | copy-start | bytes 786436
  197.9 2.7 %copy-start.6 = (bf16[192,512]{1,0:T(8,128)(2,1)S(1)}, bf16[192,512]{1,0:T(8,128)(2,1)}, u32[]{:S(2)}) copy-start(bf16[192,512]{1,0:T(8,128)(2,1)} %param.15) | copy-start | bytes 589828
  206.1 3.2 %copy-start.21 = (bf16[8,192,256]{2,1,0:T(8,128)(2,1)S(1)}, bf16[8,192,256]{2,1,0:T(8,128)(2,1)}, u32[]{:S(2)}) copy-start(bf16[8,192,256]{2,1,0:T(8,128)(2,1)} %get-tuple-element.19) | copy-start | bytes 2359300
  206.7 2.6 %copy-start.19 = (bf16[8,192,512]{2,1,0:T(8,128)(2,1)S(1)}, bf16[8,192,512]{2,1,0:T(8,128)(2,1)}, u32[]{:S(2)}) copy-start(bf16[8,192,512]{2,1,0:T(8,128)(2,1)} %get-tuple-element.20) | copy-start | bytes 4718596
  207.1 3.6 %copy-start.12 = (f32[2,384,256]{2,1,0:T(8,128)S(1)}, f32[2,384,256]{2,1,0:T(8,128)}, u32[]{:S(2)}) copy-start(f32[2,384,256]{2,1,0:T(8,128)} %copy-done.11) | copy-start | bytes 2359300
  207.9 2.8 %copy-start.8 = (bf16[2,8,48,2048]{3,2,1,0:T(8,128)(2,1)S(1)}, bf16[2,8,48,2048]{3,2,1,0:T(8,128)(2,1)}, u32[]{:S(2)}) copy-start(bf16[2,8,48,2048]{3,2,1,0:T(8,128)(2,1)} %get-tuple-element.17) | copy-start | bytes 9437188
  207.9 2.8 %copy-start.10 = (f32[2,384,256]{2,1,0:T(8,128)S(1)}, f32[2,384,256]{2,1,0:T(8,128)}, u32[]{:S(2)}) copy-start(f32[2,384,256]{2,1,0:T(8,128)} %copy-done.9) | copy-start | bytes 2359300
  210.7 3.4 %copy-start.2 = (bf16[2,8,48,2048]{3,2,1,0:T(8,128)(2,1)S(1)}, bf16[2,8,48,2048]{3,2,1,0:T(8,128)(2,1)}, u32[]{:S(2)}) copy-start(bf16[2,8,48,2048]{3,2,1,0:T(8,128)(2,1)} %get-tuple-element.16) | copy-start | bytes 9437188
  210.7 3.4 %copy-start.18 = (bf16[2,384,256]{2,1,0:T(8,128)(2,1)S(1)}, bf16[2,384,256]{2,1,0:T(8,128)(2,1)}, u32[]{:S(2)}) copy-start(bf16[2,384,256]{2,1,0:T(8,128)(2,1)} %copy-done.17) | copy-start | bytes 1179652
  214.1 3.5 %copy-start.16 = (bf16[2,384,256]{2,1,0:T(8,128)(2,1)S(1)}, bf16[2,384,256]{2,1,0:T(8,128)(2,1)}, u32[]{:S(2)}) copy-start(bf16[2,384,256]{2,1,0:T(8,128)(2,1)} %copy-done.15) | copy-start | bytes 1179652
